TPU v7x, 256 devices: a whole 4x4x8 slice. The times are simulated.
256 devices in a mesh: sp: 32 (over z, y), tp: 8 (over x, core).
Axes of the slice: x: 4, y: 4, z: 8, core: 2. Of those that a mesh axis runs over, the one named last changes fastest.
Arguments:
- tokens: bfloat16 [4, 16384, 2048], P(None, ('sp', 'tp')), may hold values from -6 to 6
- in_gain: float32 [2048], replicated, may hold values from 0.1 to 1.9
- query_weight: bfloat16 [2048, 1024], P(None, 'tp'), may hold values from -0.125 to 0.125
- key_weight: bfloat16 [2048, 1024], P(None, 'tp'), may hold values from -0.125 to 0.125
- value_weight: bfloat16 [2048, 1024], P(None, 'tp'), may hold values from -0.125 to 0.125
- gate_weight: bfloat16 [2048, 1024], P(None, 'tp'), may hold values from -0.125 to 0.125
- log_decay: float32 [8], P('tp'), may hold values from -0.034 to 0, as said below
- norm_gain: float32 [1024], P('tp'), may hold values from 0.1 to 1.9
- out_weight: bfloat16 [1024, 2048], replicated, may hold values from -0.1875 to 0.1875
- post_gain: float32 [2048], replicated, may hold values from 0.1 to 1.9
Outputs:
- mixed: bfloat16 [4, 16384, 2048], P(None, ('sp', 'tp'))
Inputs may be any that keep to these rules, and one draw needn't show every extreme that they name: `log_decay`: every entry is negative; some heads keep a tenth or more of their memory over 16384 positions, others lose most of it within 30 to 100 positions.
All inputs are finite; a program needn't handle non-finite values.
Results may differ from a plain program's by a relative error of at most 0.015.
Values may be sent and summed in bfloat16 or wider, within the bound.
A program may use at most 64 MiB of HBM per device.

v0:
```python
import jax
import jax.numpy as jnp
from jax import lax
from jax.sharding import Mesh
from jax.sharding import PartitionSpec as P

HEAD_DIM = 128
BLOCK = 128
SP = ("sp_0", "sp_1")
SP_TP = ("sp_0", "sp_1", "tp")


rms_eps = 1e-06
group_eps = 1e-05
rope_base = 10000.0


def neutral_like(shard, identity):
    return jax.tree.map(
        lambda part, zero: jnp.zeros_like(part) + jnp.asarray(zero, part.dtype), shard, identity
    )


def entering(shard, axes, combine, identity):
    before = start = neutral_like(shard, identity)
    running = shard
    for axis in reversed(axes):
        length, mine = (lax.axis_size(axis), lax.axis_index(axis))
        pieces = jax.tree.map(lambda part: lax.all_gather(part, axis), running)
        inside, running = (start, start)
        for k in range(length):
            passed = k < mine
            running = combine(running, jax.tree.map(lambda part: part[k], pieces))
            inside = jax.tree.map(lambda new, old: jnp.where(passed, new, old), running, inside)
        before = combine(inside, before)
    return before


def rotate(values, positions):
    half_dim = values.shape[-1] // 2
    inverse = rope_base ** (-jnp.arange(half_dim, dtype=jnp.float32) / half_dim)
    angles = positions.astype(jnp.float32)[:, None] * inverse[None, :]
    cosine = jnp.cos(angles)
    sine_part = jnp.sin(angles)
    first_half = values[..., :half_dim].astype(jnp.float32)
    second = values[..., half_dim:].astype(jnp.float32)
    return jnp.concatenate(
        [first_half * cosine - second * sine_part, first_half * sine_part + second * cosine],
        axis=-1,
    )


def local_pass(queries, key_rows, values, log_decay):
    seq_count, head_count, length, head_width = queries.shape
    block_count = length // BLOCK
    offsets = jnp.arange(BLOCK, dtype=jnp.float32)
    distance = offsets[:, None] - offsets[None, :]
    rate_col = log_decay[:, None, None]
    inside = jnp.where(distance >= 0, jnp.exp(rate_col * jnp.maximum(distance, 0.0)), 0.0)
    query_scale = jnp.exp(log_decay[:, None] * (offsets + 1.0))[..., None]
    key_scale = jnp.exp(log_decay[:, None] * (BLOCK - 1.0 - offsets))[..., None]
    block_decay = jnp.exp(log_decay * BLOCK)[:, None, None]

    def to_blocks(arr):
        return arr.reshape(seq_count, head_count, block_count, BLOCK, arr.shape[-1]).transpose(
            2, 0, 1, 3, 4
        )

    def advance(memory, inputs):
        q_block, k_block, v_block = inputs
        scores = jnp.einsum("shqd,shkd->shqk", q_block, k_block, preferred_element_type=jnp.float32)
        weights = (scores * inside).astype(jnp.bfloat16)
        within = jnp.einsum("shqk,shkv->shqv", weights, v_block, preferred_element_type=jnp.float32)
        carried = jnp.einsum("shqd,shdv->shqv", q_block.astype(jnp.float32) * query_scale, memory)
        k_scaled = (k_block.astype(jnp.float32) * key_scale).astype(jnp.bfloat16)
        memory = memory * block_decay + jnp.einsum(
            "shkd,shkv->shdv", k_scaled, v_block, preferred_element_type=jnp.float32
        )
        return (memory, within + carried)

    start_memory = jnp.zeros((seq_count, head_count, head_width, values.shape[-1]), jnp.float32)
    end_state, outputs = lax.scan(
        advance, start_memory, (to_blocks(queries), to_blocks(key_rows), to_blocks(values))
    )
    outputs = outputs.transpose(1, 2, 0, 3, 4).reshape(
        seq_count, head_count, length, values.shape[-1]
    )
    return (outputs, end_state)


def combine(earlier, later_part):
    return (
        earlier[0] * later_part[0],
        earlier[1] * later_part[0][None, :, None, None] + later_part[1],
    )


def read_out(carried, queries, partial_out, log_decay):
    length = queries.shape[2]
    read_scale = jnp.exp(log_decay[:, None] * (jnp.arange(length, dtype=jnp.float32) + 1.0))[
        ..., None
    ]
    return partial_out + jnp.einsum(
        "shld,shdv->shlv", queries.astype(jnp.float32) * read_scale, carried
    )


def body(
    tokens,
    in_gain,
    query_weight,
    key_weight,
    value_weight,
    gate_weight,
    log_decay,
    norm_gain,
    out_weight,
    post_gain,
):
    seq_count, rows_dev, model_width = tokens.shape
    tp_size = lax.axis_size("tp")
    local_width = query_weight.shape[1]
    head_count = local_width // HEAD_DIM
    stretch = rows_dev * tp_size
    tok_f32 = tokens.astype(jnp.float32)
    normed = (
        tok_f32 * lax.rsqrt(jnp.mean(tok_f32 * tok_f32, axis=-1, keepdims=True) + rms_eps) * in_gain
    ).astype(jnp.bfloat16)
    joined = jnp.concatenate([query_weight, key_weight, value_weight, gate_weight], axis=1)
    projected = jnp.einsum(
        "kux,xt->kut",
        lax.all_gather(normed, "tp", axis=1, tiled=True),
        joined,
        preferred_element_type=jnp.float32,
    ).astype(jnp.bfloat16)

    def heads_of(columns):
        return columns.reshape(seq_count, stretch, head_count, HEAD_DIM).transpose(0, 2, 1, 3)

    positions = lax.axis_index(SP) * stretch + jnp.arange(stretch, dtype=jnp.int32)
    queries = rotate(heads_of(projected[..., :local_width]), positions).astype(jnp.bfloat16)
    key_rows = (
        rotate(heads_of(projected[..., local_width : 2 * local_width]), positions)
        * HEAD_DIM ** (-0.5)
    ).astype(jnp.bfloat16)
    values = heads_of(projected[..., 2 * local_width : 3 * local_width])
    gating = projected[..., 3 * local_width :]
    partial_out, end_state = local_pass(queries, key_rows, values, log_decay)
    span_decay = jnp.exp(log_decay * stretch)
    carried = entering(
        (span_decay, end_state), SP, combine, (jnp.ones_like(span_decay), jnp.zeros_like(end_state))
    )[1]
    retained = read_out(carried, queries, partial_out, log_decay)
    center = jnp.mean(retained, axis=-1, keepdims=True)
    spread = jnp.mean(jnp.square(retained - center), axis=-1, keepdims=True)
    normal = (
        ((retained - center) * lax.rsqrt(spread + group_eps))
        .transpose(0, 2, 1, 3)
        .reshape(seq_count, stretch, local_width)
    )
    gated = (normal * norm_gain * jax.nn.silu(gating.astype(jnp.float32))).astype(jnp.bfloat16)
    premix = jnp.einsum(
        "hor,rn->hon",
        lax.all_to_all(gated, "tp", split_axis=1, concat_axis=2, tiled=True),
        out_weight,
        preferred_element_type=jnp.float32,
    )
    mixed = (
        premix * lax.rsqrt(jnp.mean(premix * premix, axis=-1, keepdims=True) + rms_eps) * post_gain
    )
    return mixed.astype(jnp.bfloat16)


def solution(mesh):
    torus = Mesh(mesh.devices.reshape(8, 4, mesh.shape["tp"]), ("sp_0", "sp_1", "tp"))
    return jax.shard_map(
        body,
        mesh=torus,
        in_specs=(
            P(None, SP_TP, None),
            P(),
            P(None, "tp"),
            P(None, "tp"),
            P(None, "tp"),
            P(None, "tp"),
            P("tp"),
            P("tp"),
            P(),
            P(),
        ),
        out_specs=P(None, SP_TP, None),
        check_vma=False,
    )
```

profile of v0, /device:TPU:1, one launch (start us, length us, event | category | flops | bytes accessed | tf_op | source)
XLA Modules:
  0.0 204.7 jit_solution(9332395953188734523)
XLA Ops:
  6.5 1.6 fusion.44
  8.1 2.6 %fusion.46 = bf16[4,64,2048]{2,1,0:T(8,128)(2,1)} fusion(bf16[4,64,2048]{2,1,0:T(8,128)(2,1)} %param.12, f32[2048]{0:T(1024)} %param.13, f32[4,64]{1,0:T(4,128)S(1)} %add_rsqrt_fusion.2), kind=kLoop, calls=%fused_computation.48 | loop fusion | flops 2097152 | bytes 2106368 | tf_op jit(solution)/shard_map/convert_element_type | solution.py:128
  10.9 0.2 copy.39
  11.1 0.2 copy.40
  11.3 0.5 copy-done.10
  11.8 0.2 copy.41
  12.0 0.2 copy.42
  13.0 0.5 multiply_cosine_fusion
  13.5 53.8 %all-gather.7.cloned.1.call-done = bf16[4,512,2048]{2,1,0:T(8,128)(2,1)} async-done(((bf16[4,64,2048]{2,1,0:T(8,128)(2,1)}), bf16[4,512,2048]{2,1,0:T(8,128)(2,1)}) %all-gather.7.cloned.1.call-update) | async-done | bytes 8388624 | tf_op jit(solution)/shard_map/all_gather | solution.py:132
  67.3 9.5 %fusion.54 = bf16[4,512,512]{1,2,0:T(8,128)(2,1)S(1)} fusion(bf16[4,512,2048]{2,1,0:T(8,128)(2,1)} %all-gather.7.cloned.1.call-done, bf16[2048,128]{0,1:T(8,128)(2,1)S(1)} %copy.42, bf16[2048,128]{0,1:T(8,128)(2,1)S(1)} %copy.41, bf16[2048,128]{0,1:T(8,128)(2,1)S(1)} %copy.40, bf16[2048,128]{0,1:T(8,128)(2,1)S(1)} %copy.39), kind=kOutput, calls=%fused_computation.59 | convolution fusion | flops 4304404480 | bytes 12582912 | tf_op jit(solution)/shard_map/kux,xt->kut/dot_general | solution.py:130
  76.9 1.0 slice_bitcast_fusion
  77.9 0.3 fusion.66
  78.4 0.3 copy.46
  78.8 0.3 copy-done.6
  79.3 0.3 copy.47
  79.8 0.3 copy.43
  80.3 1.3 copy.44
  81.6 1.2 reshape_transpose_reshape.3
  82.8 0.4 copy.45
  83.2 0.3 maximum_bitcast_fusion.4
  83.5 0.9 copy-done.1
  84.4 0.3 fusion.69
  84.8 11.9 %while.15 = (s32[]{:T(128)}, f32[4,1,128,128]{3,2,0,1:T(8,128)S(1)}, f32[4,4,1,128,128]{4,3,1,2,0:T(8,128)}, f32[1]{0:T(128)}, bf16[4,4,1,128,128]{4,3,1,2,0:T(8...) while((s32[]{:T(128)}, ...), condition=%wide.region_2.3_spmd.clone.clone.clone, body=%wide.region_1.2_spmd.clone.clone.clone.sunk | while | flops 67977728 | bytes 2496632 | solution.py:82
  84.8 0.7 select_bitcast_fusion.2
  85.5 0.3 fusion.146
  85.9 0.7 exponential_bitcast_fusion.3
  86.5 0.9 fusion.147
  87.5 0.3 fusion.145
  87.8 0.7 select_bitcast_fusion.2
  88.5 0.3 fusion.146
  88.8 0.7 exponential_bitcast_fusion.3
  89.5 0.9 fusion.147
  90.4 0.3 fusion.145
  90.8 0.7 select_bitcast_fusion.2
  91.5 0.3 fusion.146
  91.8 0.7 exponential_bitcast_fusion.3
  92.5 0.9 fusion.147
  93.4 0.3 fusion.145
  93.8 0.7 select_bitcast_fusion.2
  94.5 0.3 fusion.146
  94.8 0.7 exponential_bitcast_fusion.3
  95.5 0.9 fusion.147
  96.4 0.3 fusion.145
  96.8 0.7 copy-done
  97.5 0.6 dynamic-slice
  98.1 0.7 exponential_dynamic-update-slice_fusion
  98.8 8.4 %all-reduce = f32[4]{0:T(128)S(1)} all-reduce(f32[4]{0:T(128)S(1)} %exponential_dynamic-update-slice_fusion), channel_id=2, replica_groups=mesh['sp_0'=8,'sp_1'=4,'tp'=8] {'sp_1'}, use_global_device_ids=true, to_apply=%add | all-reduce | flops 4 | bytes 32
  107.2 0.7 slice_multiply_fusion.1
  107.9 1.3 slice_multiply_fusion
  109.9 12.2 %all-gather.11.cloned.1.call-done = f32[16,1,128,128]{3,2,1,0:T(8,128)} async-done(((f32[4,1,128,128]{3,2,1,0:T(8,128)}), f32[16,1,128,128]{3,2,1,0:T(8,128)}) %all-gather.11.cloned.1.call-update) | async-done | bytes 1048592 | tf_op jit(solution)/shard_map/all_gather | solution.py:29
  122.0 3.8 %slice_add_fusion.8 = f32[4,1,128,128]{3,2,1,0:T(8,128)} fusion(f32[16,1,128,128]{3,2,1,0:T(8,128)} %all-gather.11.cloned.1.call-done, f32[]{:T(128)} %bitcast.20, f32[]{:T(128)} %bitcast.18, f32[16,1,128,128]{3,2,0,1:T(8,128)} %bitcast.197, f32[]{:T(128)} %bitcast.16, f32[]{:T(128)} %bitcast.13), kind=kLoop, calls=%fused_computation.109 | loop fusion | flops 458752 | bytes 1310736 | tf_op jit(solution)/shard_map/add | solution.py:94
  125.9 0.6 dynamic-slice.1
  126.4 1.3 dynamic-update-slice.1
  127.7 13.9 %all-reduce.1 = f32[8]{0:T(128)S(1)} all-reduce(f32[8]{0:T(128)S(1)} %dynamic-update-slice.1), channel_id=3, replica_groups=mesh['sp_0'=8,'sp_1'=4,'tp'=8] {'sp_0'}, use_global_device_ids=true, to_apply=%add.1 | all-reduce | flops 8 | bytes 64
  141.6 0.7 fusion.127
  145.5 0.4 copy.48
  145.9 0.4 reshape.499
  146.3 18.7 %all-gather.9.cloned.1.call-done = f32[8,4,1,128,128]{4,3,2,1,0:T(8,128)} async-done(((f32[1,4,1,128,128]{4,3,2,1,0:T(8,128)}), f32[8,4,1,128,128]{4,3,2,1,0:T(8,128)}) %all-gather.9.cloned.1.call-update) | async-done | bytes 2097168 | tf_op jit(solution)/shard_map/all_gather | solution.py:29
  165.1 7.9 %fusion.128 = (f32[4,512]{1,0:T(4,128)S(1)}, f32[4,512,128]{1,2,0:T(8,128)S(1)}) fusion(f32[4,512,128]{1,2,0:T(8,128)S(1)} %reshape.499, f32[8,4,1,128,128]{4,3,1,2,0:T(8,128)} %bitcast.204, f32[4,1,128,128]{3,2,1,0:T(8,128)S(1)} %copy-done.4, f32[16,1,128,128]{3,2,0,1:T(8,128)S(1)} %bitcast.198, f32[16,1,128,128]{3,2,1,0:T(8,128)S(1)} %copy-done.3, ...), kind=kOutput, calls=%fused_computation.175 | convolution fusion | flops 71170048 | bytes 5777468 | tf_op jit(solution)/shard_map/shld,shdv->shlv/dot_general | solution.py:103
  173.2 1.5 fusion.62
  174.7 0.3 copy.65
  175.0 18.3 %all_to_all.18 = bf16[4,512,128]{2,0,1:T(4,128)(2,1)S(1)} all-to-all(bf16[4,512,128]{2,0,1:T(4,128)(2,1)S(1)} %copy.65), channel_id=1, replica_groups=mesh['sp_0'=8,'sp_1'=4,'tp'=8] {'tp'}, dimensions={1} | all-to-all | bytes 1048576 | tf_op jit(solution)/shard_map/all_to_all | solution.py:164
  193.4 3.6 %multiply_reduce_fusion = (f32[4,64]{1,0:T(4,128)S(1)}, f32[4,64,2048]{2,1,0:T(8,128)S(1)}) fusion(bf16[1024,2048]{1,0:T(8,128)(2,1)} %param.20, bf16[4,8,8,8,128]{4,3,2,1,0:T(8,128)(2,1)S(1)} %bitcast.203), kind=kOutput, calls=%fused_computation.58 | convolution fusion | flops 1074790144 | bytes 6816768 | tf_op jit(solution)/shard_map/hor,rn->hon/dot_general | solution.py:162
  197.0 1.2 multiply_convert_fusion.2
  (51 shorter events, 1.3 us)
Async XLA Ops:
  6.5 4.3 %copy-start.8 = (bf16[2048,128]{1,0:T(8,128)(2,1)S(1)}, bf16[2048,128]{1,0:T(8,128)(2,1)}, u32[]{:S(2)}) copy-start(bf16[2048,128]{1,0:T(8,128)(2,1)} %param.14) | copy-start | bytes 1572868
  6.5 60.8 %all-gather.7.cloned.1.call-start = ((), (), s32[]{:S(2)}) async-start(), calls=%async_computation.1 | async-start | bytes 9437184 | tf_op jit(solution)/shard_map/all_gather | solution.py:132
  8.1 3.0 %copy-start.9 = (bf16[2048,128]{1,0:T(8,128)(2,1)S(1)}, bf16[2048,128]{1,0:T(8,128)(2,1)}, u32[]{:S(2)}) copy-start(bf16[2048,128]{1,0:T(8,128)(2,1)} %param.15) | copy-start | bytes 1572868
  10.8 1.0 copy-start.10
  10.8 1.3 copy-start.11
  10.8 111.2 %all-gather.11.cloned.1.call-start = ((), (), s32[]{:S(2)}) async-start(), calls=%async_computation.3 | async-start | bytes 1310720 | tf_op jit(solution)/shard_map/all_gather | solution.py:29
  76.9 1.5 copy-start.2
  78.3 0.7 copy-start.6
  78.4 0.8 copy-start.7
  83.2 1.2 copy-start.1
  84.8 12.8 %copy-start.15 = (u32[256]{0:T(256)S(1)}, u32[256]{0:T(256)}, u32[]{:S(2)}) copy-start(u32[256]{0:T(256)} %constant.86) | copy-start | bytes 3076
  84.8 41.1 %copy-start.14 = (u32[256]{0:T(256)S(1)}, u32[256]{0:T(256)}, u32[]{:S(2)}) copy-start(u32[256]{0:T(256)} %constant.91) | copy-start | bytes 3076
  96.7 0.7 copy-start
  96.7 48.7 %copy-start.5 = (f32[4,4,1,128,128]{4,3,1,2,0:T(8,128)S(1)}, f32[4,4,1,128,128]{4,3,1,2,0:T(8,128)}, u32[]{:S(2)}) copy-start(f32[4,4,1,128,128]{4,3,1,2,0:T(8,128)} %get-tuple-element.58) | copy-start | bytes 3145732
  97.5 67.6 %all-gather.9.cloned.1.call-start = ((), (), s32[]{:S(2)}) async-start(), calls=%async_computation.2 | async-start | bytes 2359296 | tf_op jit(solution)/shard_map/all_gather | solution.py:29
  145.5 19.6 %copy-start.3 = (f32[16,1,128,128]{3,2,1,0:T(8,128)S(1)}, f32[16,1,128,128]{3,2,1,0:T(8,128)}, u32[]{:S(2)}) copy-start(f32[16,1,128,128]{3,2,1,0:T(8,128)} %all-gather.11.cloned.1.call-done) | copy-start | bytes 3145732
  145.5 19.6 %copy-start.4 = (f32[4,1,128,128]{3,2,1,0:T(8,128)S(1)}, f32[4,1,128,128]{3,2,1,0:T(8,128)}, u32[]{:S(2)}) copy-start(f32[4,1,128,128]{3,2,1,0:T(8,128)} %slice_add_fusion.8) | copy-start | bytes 786436
  165.1 8.1 %copy-start.13 = (f32[128]{0:T(128)S(1)}, f32[128]{0:T(128)}, u32[]{:S(2)}) copy-start(f32[128]{0:T(128)} %param.19) | copy-start | bytes 1540
  193.4 3.6 %copy-start.12 = (f32[2048]{0:T(1024)S(1)}, f32[2048]{0:T(1024)}, u32[]{:S(2)}) copy-start(f32[2048]{0:T(1024)} %param.21) | copy-start | bytes 24580
Sparse Core Ops, SparseCore 0:
  10.9 56.3 all-gather.6
  97.6 24.3 all-gather.10
  126.0 39.0 all-gather.8
where the time goes:
time: 205 us
  waiting for transfers between devices  84.8 us (41%)
  blocking collectives  40.6 us (20%)
  matrix products  27.4 us (13%)
  other arithmetic  20.4 us (10%)
  between operations  18 us (9%)
  local copies, waits for them, and re-layouts  13.3 us (6%)
    all_gather x1, waiting for transfers between devices, body(): lax.all_gather(normed, 'tp', axis=1, tiled=True)  53.8 us
    all_gather x2, waiting for transfers between devices, entering(): pieces = jax.tree.map(lambda part: lax.all_gather(part, axis), running)  30.9 us
    unnamed x2, blocking collectives  22.3 us
    all_to_all x1, blocking collectives, body(): lax.all_to_all(gated, 'tp', split_axis=1, concat_axis=2, tiled=True)  18.3 us
    dot_general x1, matrix products, body(): jnp.einsum('kux,xt->kut', lax.all_gather(normed, 'tp', axis=1, tiled=True...  9.51 us
    dot_general x1, matrix products, read_out(): jnp.einsum('shld,shdv->shlv', queries.astype(jnp.float32) * read_scale, c...  7.93 us
    unnamed x41, local copies, waits for them, and re-layouts  6.03 us
  transfers between devices with their start and end apart: 3, of which 3 were waited for; matrix products, arithmetic and copies ran while one was open for 4% of the time, Pallas kernels for 0%

commit v1 on v0

v1 whole, which is shorter than its diff:
```python
import functools

import jax
import jax.numpy as jnp
import numpy as np
from jax import lax
from jax.experimental import pallas as pl
from jax.experimental.pallas import tpu as pltpu
from jax.sharding import PartitionSpec as P

MESH = pl.DeviceIdType.MESH
F32 = jnp.float32
BF16 = jnp.bfloat16
HD = 128
BLOCK = 128
NY = 4
RMS_EPS = 1e-06
GROUP_EPS = 1e-05
ROPE_BASE = 10000.0


def rotary_tables(blocks):
    half = HD // 2
    rate = ROPE_BASE ** (-np.arange(half, dtype=np.float64) / half)
    rate = np.concatenate([rate, rate])
    inside = np.arange(BLOCK, dtype=np.float64)[:, None] * rate
    starts = BLOCK * np.arange(blocks, dtype=np.float64)[:, None] * rate
    tables = (np.cos(inside), np.sin(inside), np.cos(starts), np.sin(starts))
    return [t.astype(np.float32) for t in tables]


def kernel(
    nz, ny, tok_hbm, gain, wq, wk, wv, wg, ld_ref, ng, ow, pg, cin, sin_, cbl, sbl, out_ref,
    raw, tok, w, oww, ctab, stab, dmat, qsc, ksc, qs, acc, gs, smat, esend, ybuf, zsnd, zbuf, msnd, mbuf,
    gsend, gat, osc, lsem, xs, xr, rs, rr, ps, pr, ys, yr, zs, zr, ms, mr, as_, ar,
):
    nseq, rows, width = raw.shape
    ntp = 8
    nchip = ntp // 2
    hr = rows // 2
    qr = HD // ny
    sp = lax.axis_index("sp")
    me = lax.axis_index("tp")
    z, y = sp // ny, sp % ny
    chip, core = me // 2, me % 2
    partner = chip * 2 + 1 - core
    left_chip, right_chip, far_chip = (chip + 3) % nchip, (chip + 1) % nchip, (chip + 2) % nchip
    left, right, far = left_chip * 2 + core, right_chip * 2 + core, far_chip * 2 + core

    barrier = pltpu.get_barrier_semaphore()
    peers = [(sp, (me + k) % ntp) for k in range(1, ntp)]
    peers += [(z * ny + (y + k) % ny, me) for k in range(1, ny)]
    peers += [((z + k) % nz * ny + y, me) for k in range(1, nz)]
    for dev in peers:
        pl.semaphore_signal(barrier, inc=1, device_id=dev, device_id_type=MESH)

    loads = [pltpu.make_async_copy(tok_hbm, raw, lsem.at[0])]
    for j, src in enumerate((wq, wk, wv, wg)):
        loads.append(pltpu.make_async_copy(src, w.at[:, j * HD:(j + 1) * HD], lsem.at[1 + j]))
    loads.append(pltpu.make_async_copy(ow, oww, lsem.at[5]))
    for load in loads:
        load.start()

    def remote(src, dst, send, recv, dev):
        return pltpu.make_async_remote_copy(
            src_ref=src, dst_ref=dst, send_sem=send, recv_sem=recv, device_id=dev, device_id_type=MESH
        )

    def piece(s, d, lo, n):
        return tok.at[s, pl.ds(pl.multiple_of(d * rows + lo, hr), n), :]

    halves = (0, hr, hr, 0)

    def own_send(s, i):
        ref = piece(s, me, halves[i], hr)
        return remote(ref, ref, xs.at[s, i], xr.at[s, i], (sp, (right, right, left, left)[i]))

    def own_recv(s, i):
        ref = piece(s, (left, left, right, right)[i], halves[i], hr)
        return remote(ref, ref, xs.at[s, i], xr.at[s, i], (sp, right))

    def relay_send(s, i):
        ref = piece(s, (left, right)[i], i * hr, hr)
        return remote(ref, ref, rs.at[s, i], rr.at[s, i], (sp, (right, left)[i]))

    def relay_recv(s, i):
        ref = piece(s, far, i * hr, hr)
        return remote(ref, ref, rs.at[s, i], rr.at[s, i], (sp, right))

    same = (me, left, right, far)
    other = tuple(chip_ * 2 + 1 - core for chip_ in (chip, left_chip, right_chip, far_chip))

    def pair_send(s, i):
        ref = piece(s, same[i], 0, rows)
        return remote(ref, ref, ps.at[s, i], pr.at[s, i], (sp, partner))

    def pair_recv(s, i):
        ref = piece(s, other[i], 0, rows)
        return remote(ref, ref, ps.at[s, i], pr.at[s, i], (sp, partner))

    def ycopy(s, to):
        src = esend.at[s, pl.ds(pl.multiple_of(to * qr, qr), qr), :]
        return remote(src, ybuf.at[s, y], ys.at[s, to], yr.at[s, y], (z * ny + to, me))

    def yrecv(s, frm):
        ref = ybuf.at[s, frm]
        return remote(ref, ref, ys.at[s, frm], yr.at[s, frm], (z * ny + frm, me))

    def zcopy(s, to):
        return remote(zsnd.at[s], zbuf.at[s, z], zs.at[s, to], zr.at[s, z], (to * ny + y, me))

    def zrecv(s, frm):
        ref = zbuf.at[s, frm]
        return remote(ref, ref, zs.at[s, frm], zr.at[s, frm], (frm * ny + y, me))

    def mcopy(s, to):
        dst = mbuf.at[s, pl.ds(pl.multiple_of(y * qr, qr), qr), :]
        return remote(msnd.at[s, to], dst, ms.at[s, to], mr.at[s, y], (z * ny + to, me))

    def mrecv(s, frm):
        ref = mbuf.at[s, pl.ds(pl.multiple_of(frm * qr, qr), qr), :]
        return remote(ref, ref, ms.at[s, frm], mr.at[s, frm], (z * ny + frm, me))

    def acopy(s, to):
        src = gsend.at[s, pl.ds(pl.multiple_of(to * rows, rows), rows), :]
        dst = gat.at[s, :, pl.ds(pl.multiple_of(me * HD, HD), HD)]
        return remote(src, dst, as_.at[s, to], ar.at[s, me], (sp, to))

    def arecv(s, frm):
        ref = gat.at[s, :, pl.ds(pl.multiple_of(frm * HD, HD), HD)]
        return remote(ref, ref, as_.at[s, frm], ar.at[s, frm], (sp, frm))

    ld = ld_ref[0]
    i_col = lax.broadcasted_iota(jnp.int32, (BLOCK, HD), 0).astype(F32)
    i_row = lax.broadcasted_iota(jnp.int32, (BLOCK, HD), 1).astype(F32)
    dist = i_col - i_row
    dmat[...] = jnp.where(dist >= 0, jnp.exp(ld * jnp.maximum(dist, 0.0)), 0.0)
    qsc[...] = jnp.exp(ld * (i_col + 1.0))
    ksc[...] = jnp.exp(ld * (BLOCK - 1.0 - i_col))
    sign = jnp.where(i_row < HD // 2, -1.0, 1.0)

    def decay(count):
        return jnp.exp(jnp.full((1, HD), ld * count, F32))

    @pl.loop(0, nchip)
    def _(b):
        block = sp * nchip + b
        cb = cbl[pl.ds(block, 1), :]
        sb = sbl[pl.ds(block, 1), :]
        ctab[b] = cin[...] * cb - sin_[...] * sb
        stab[b] = (sin_[...] * cb + cin[...] * sb) * sign

    loads[0].wait()
    part = 16

    @pl.loop(0, nseq * (rows // part))
    def _(t):
        s, c = t // (rows // part), t % (rows // part)
        v = raw[s, pl.ds(pl.multiple_of(c * part, part), part), :].astype(F32)
        scale = lax.rsqrt(jnp.mean(v * v, axis=-1, keepdims=True) + RMS_EPS)
        at = pl.multiple_of(me * rows + c * part, part)
        tok[s, pl.ds(at, part), :] = (v * scale * gain[...]).astype(BF16)

    pl.semaphore_wait(barrier, len(peers))

    def start_own(s):
        for i in (0, 2, 1, 3):
            own_send(s, i).start()
        pair_send(s, 0).start()

    start_own(0)
    for load in loads[1:]:
        load.wait()

    def rotate(u, b):
        return u * ctab[b] + pltpu.roll(u, HD // 2, 1) * stab[b]

    def block_work(s, b):
        at = pl.ds(pl.multiple_of(b * BLOCK, BLOCK), BLOCK)
        proj = jnp.dot(tok[s, at, :], w[...], preferred_element_type=F32).astype(BF16)
        q = rotate(proj[:, :HD].astype(F32), b).astype(BF16)
        k = (rotate(proj[:, HD:2 * HD].astype(F32), b) * HD ** -0.5).astype(BF16)
        v = proj[:, 2 * HD:3 * HD]
        g = proj[:, 3 * HD:].astype(F32)
        scores = lax.dot_general(q, k, (((1,), (1,)), ((), ())), preferred_element_type=F32)
        weights = (scores * dmat[...]).astype(BF16)
        acc[s, at, :] = jnp.dot(weights, v, preferred_element_type=F32)
        qs[s, at, :] = (q.astype(F32) * qsc[...]).astype(BF16)
        ks = (k.astype(F32) * ksc[...]).astype(BF16)
        smat[b] = lax.dot_general(ks, v, (((0,), (0,)), ((), ())), preferred_element_type=F32)
        gs[s, at, :] = ng[...] * (g * jax.nn.sigmoid(g))

    def state_out(s):
        step = decay(float(BLOCK))
        prefix = smat[0]
        befores = []
        for b in range(1, nchip):
            befores.append(prefix.astype(BF16))
            prefix = prefix * step + smat[b]
        esend[s] = prefix.astype(BF16)
        ybuf[s, y] = esend[s, pl.ds(pl.multiple_of(y * qr, qr), qr), :]
        for k in range(1, ny):
            ycopy(s, (y + k) % ny).start()
        for b in range(1, nchip):
            at = pl.ds(b * BLOCK, BLOCK)
            acc[s, at, :] += jnp.dot(qs[s, at, :], befores[b - 1], preferred_element_type=F32)

    def state_row(s):
        for k in range(1, ny):
            yrecv(s, (y + k) % ny).wait_recv()
        span = decay(float(BLOCK * nchip))
        total = ybuf[s, 0].astype(F32)
        for k in range(1, ny):
            total = total * span + ybuf[s, k].astype(F32)
        zsnd[s] = total.astype(BF16)

        @pl.loop(z + 1, nz)
        def _(to):
            zcopy(s, to).start()

    def state_back(s):
        span = decay(float(BLOCK * nchip))
        row_span = decay(float(BLOCK * nchip * ny))

        def add(frm, total):
            zrecv(s, frm).wait_recv()
            return total * row_span + zbuf[s, frm].astype(F32)

        carried = lax.fori_loop(0, z, add, jnp.zeros((qr, HD), F32))
        for k in range(ny):
            msnd[s, k] = carried.astype(BF16)
            if k < ny - 1:
                carried = carried * span + ybuf[s, k].astype(F32)
        mbuf[s, pl.ds(pl.multiple_of(y * qr, qr), qr), :] = msnd[s, y]
        for k in range(1, ny):
            mcopy(s, (y + k) % ny).start()

    def read_out(s):
        for k in range(1, ny):
            mrecv(s, (y + k) % ny).wait_recv()
        memory = mbuf[s]
        for b in range(nchip):
            at = pl.ds(b * BLOCK, BLOCK)
            kept = jnp.dot(qs[s, at, :], memory, preferred_element_type=F32)
            kept = acc[s, at, :] + kept * decay(float(BLOCK * b))
            kept = kept - jnp.mean(kept, axis=-1, keepdims=True)
            spread = jnp.mean(kept * kept, axis=-1, keepdims=True)
            gsend[s, at, :] = (kept * lax.rsqrt(spread + GROUP_EPS) * gs[s, at, :]).astype(BF16)
        for k in range(1, ntp):
            acopy(s, (me + k) % ntp).start()
        own = gsend[s, pl.ds(pl.multiple_of(me * rows, rows), rows), :]
        gat[s, :, pl.ds(pl.multiple_of(me * HD, HD), HD)] = own

    def mix(s):
        for k in range(1, ntp):
            arecv(s, (me + k) % ntp).wait_recv()
        osc[...] = jnp.dot(gat[s], oww[...], preferred_element_type=F32)

        @pl.loop(0, rows // part)
        def _(c):
            at = pl.ds(pl.multiple_of(c * part, part), part)
            v = osc[at, :]
            scale = lax.rsqrt(jnp.mean(v * v, axis=-1, keepdims=True) + RMS_EPS)
            out_ref[s, at, :] = (v * scale * pg[...]).astype(BF16)

    @pl.loop(0, nseq + 2)
    def _(t):
        tokens_left = t < nseq
        scanning = (t >= 1) & (t <= nseq)
        reading = t >= 2

        @pl.when(tokens_left)
        def _():
            own_recv(t, 0).wait_recv()
            relay_send(t, 0).start()
            own_recv(t, 2).wait_recv()
            relay_send(t, 1).start()

            @pl.when(t + 1 < nseq)
            def _():
                start_own(t + 1)

        @pl.when(reading)
        def _():
            read_out(t - 2)

        @pl.when(tokens_left)
        def _():
            pair_recv(t, 0).wait_recv()
            block_work(t, chip)

        @pl.when(scanning)
        def _():
            state_row(t - 1)

        @pl.when(tokens_left)
        def _():
            own_recv(t, 1).wait_recv()
            pair_send(t, 1).start()
            own_recv(t, 3).wait_recv()
            pair_send(t, 2).start()
            pair_recv(t, 1).wait_recv()
            block_work(t, left_chip)
            pair_recv(t, 2).wait_recv()
            block_work(t, right_chip)

        @pl.when(reading)
        def _():
            mix(t - 2)

        @pl.when(scanning)
        def _():
            state_back(t - 1)

        @pl.when(tokens_left)
        def _():
            relay_recv(t, 0).wait_recv()
            relay_recv(t, 1).wait_recv()
            pair_send(t, 3).start()
            pair_recv(t, 3).wait_recv()
            block_work(t, far_chip)
            state_out(t)

    @pl.loop(0, nseq)
    def _(s):
        for i in range(4):
            own_send(s, i).wait_send()
            pair_send(s, i).wait_send()
        for i in range(2):
            relay_send(s, i).wait_send()
        for k in range(1, ny):
            ycopy(s, (y + k) % ny).wait_send()
            mcopy(s, (y + k) % ny).wait_send()
        for k in range(1, ntp):
            acopy(s, (me + k) % ntp).wait_send()

        @pl.loop(z + 1, nz)
        def _(to):
            zcopy(s, to).wait_send()


def body(nz, ny, tokens, in_gain, wq, wk, wv, wg, log_decay, norm_gain, out_weight, post_gain):
    nseq, rows, width = tokens.shape
    ntp = 8
    stretch = rows * ntp
    tables = [jnp.asarray(t) for t in rotary_tables(nz * ny * stretch // BLOCK)]
    qr = HD // ny
    vmem, hbm, smem = (pl.BlockSpec(memory_space=m) for m in (pltpu.VMEM, pl.ANY, pltpu.SMEM))
    dma = pltpu.SemaphoreType.DMA
    scratch = [
        pltpu.VMEM((nseq, rows, width), BF16),
        pltpu.VMEM((nseq, stretch, width), BF16),
        pltpu.VMEM((width, 4 * HD), BF16),
        pltpu.VMEM(out_weight.shape, BF16),
        pltpu.VMEM((stretch // BLOCK, BLOCK, HD), F32),
        pltpu.VMEM((stretch // BLOCK, BLOCK, HD), F32),
        pltpu.VMEM((BLOCK, HD), F32),
        pltpu.VMEM((BLOCK, HD), F32),
        pltpu.VMEM((BLOCK, HD), F32),
        pltpu.VMEM((nseq, stretch, HD), BF16),
        pltpu.VMEM((nseq, stretch, HD), F32),
        pltpu.VMEM((nseq, stretch, HD), F32),
        pltpu.VMEM((stretch // BLOCK, HD, HD), F32),
        pltpu.VMEM((nseq, HD, HD), BF16),
        pltpu.VMEM((nseq, ny, qr, HD), BF16),
        pltpu.VMEM((nseq, qr, HD), BF16),
        pltpu.VMEM((nseq, nz, qr, HD), BF16),
        pltpu.VMEM((nseq, ny, qr, HD), BF16),
        pltpu.VMEM((nseq, HD, HD), BF16),
        pltpu.VMEM((nseq, stretch, HD), BF16),
        pltpu.VMEM((nseq, rows, ntp * HD), BF16),
        pltpu.VMEM((rows, width), F32),
        dma((6,)),
        dma((nseq, 4)), dma((nseq, 4)), dma((nseq, 2)), dma((nseq, 2)), dma((nseq, 4)), dma((nseq, 4)),
        dma((nseq, ny)), dma((nseq, ny)), dma((nseq, nz)), dma((nseq, nz)), dma((nseq, ny)), dma((nseq, ny)),
        dma((nseq, ntp)), dma((nseq, ntp)),
    ]
    return pl.pallas_call(
        functools.partial(kernel, nz, ny),
        out_shape=jax.ShapeDtypeStruct(tokens.shape, BF16),
        in_specs=[hbm, vmem, hbm, hbm, hbm, hbm, smem, vmem, hbm, vmem, vmem, vmem, vmem, vmem],
        out_specs=vmem,
        scratch_shapes=scratch,
        name="retention",
        compiler_params=pltpu.CompilerParams(
            collective_id=0, has_side_effects=True, vmem_limit_bytes=60 * 1024 * 1024
        ),
    )(
        tokens, in_gain.reshape(1, -1), wq, wk, wv, wg, log_decay, norm_gain.reshape(1, -1), out_weight,
        post_gain.reshape(1, -1), *tables,
    )


def solution(mesh):
    both = ("sp", "tp")
    nz = mesh.shape["sp"] // NY
    return jax.shard_map(
        functools.partial(body, nz, NY),
        mesh=mesh,
        in_specs=(
            P(None, both, None), P(), P(None, "tp"), P(None, "tp"), P(None, "tp"), P(None, "tp"), P("tp"), P("tp"),
            P(), P(),
        ),
        out_specs=P(None, both, None),
        check_vma=False,
    )
```

time: 205 us -> 83.2 us (0.41)
  waiting for transfers between devices: 84.8 us -> 0 us
  Pallas kernels: 0 us -> 80.1 us
  blocking collectives: 40.6 us -> 0 us
  matrix products: 27.4 us -> 0 us
  other arithmetic: 20.4 us -> 0 us
  between operations: 18 us -> 0.66 us
  local copies, waits for them, and re-layouts: 13.3 us -> 2.3 us
    all_gather x3 -> x0, waiting for transfers between devices: 84.7 us -> none  [the longest x1 53.8 us: body(): lax.all_gather(normed, 'tp', axis=1, tiled=True)]
    pallas_call x0 -> x1, Pallas kernels: none -> 80.1 us  [body(): pl.pallas_call(functools.partial(kernel, nz, ny), out_shape=jax.ShapeDtyp...]
    dot_general x15 -> x0, matrix products: 27.4 us -> none  [the longest x1 9.51 us: body(): jnp.einsum('kux,xt->kut', lax.all_gather(normed, 'tp', axis=1, tiled=True...]
    unnamed x2 -> x0, blocking collectives: 22.3 us -> none
    all_to_all x1 -> x0, blocking collectives: 18.3 us -> none  [body(): lax.all_to_all(gated, 'tp', split_axis=1, concat_axis=2, tiled=True)]
    mul x10 -> x0, other arithmetic: 7.41 us -> none  [the longest x4 2.75 us: advance(): weights = (scores * inside).astype(jnp.bfloat16)]
    convert_element_type x4 -> x0, other arithmetic: 5.33 us -> none  [the longest x1 2.65 us: body(): normed = (tok_f32 * lax.rsqrt(jnp.mean(tok_f32 * tok_f32, axis=-1, keepdi...]
    add x1 -> x0, other arithmetic: 3.78 us -> none  [combine(): earlier[1] * later_part[0][None, :, None, None] + later_part[1]]
  transfers between devices with their start and end apart: 3 -> 0, of which waited for: 3 -> 0; matrix products, arithmetic and copies ran while one was open for 4% -> 0% of each run, Pallas kernels for 0% -> 0%
where the time goes in v1:
time: 83.2 us; the launch traced here: 83.1 us
  Pallas kernels  80.1 us (96%)
  local copies, waits for them, and re-layouts  2.3 us (3%)
    pallas_call x1, Pallas kernels, body(): pl.pallas_call(functools.partial(kernel, nz, ny), out_shape=jax.ShapeDtyp...  80.1 us
    unnamed x1, local copies, waits for them, and re-layouts  2.3 us

profile of v1, /device:TPU:1, one launch (start us, length us, event | category | flops | bytes accessed | tf_op | source)
XLA Modules:
  0.0 83.1 jit_solution(9329904421764033881)
XLA Ops:
  0.7 80.1 %retention.1 = bf16[4,64,2048]{2,1,0:T(8,128)(2,1)} custom-call(bf16[4,64,2048]{2,1,0:T(8,128)(2,1)} %tok_hbm.1, f32[1,2048]{1,0:T(1,128)} %bitcast.3, bf16[2048,128]{1,0:T(8,128)(2,1)} %wq.1, bf16[2048,128]{1,0:T(8,128)(2,1)} %wk.1, bf16[2048,128]{1,0:T(8,128)(2,1)} %wv.1, bf16[2048,128]{1,0:T(8,128)(2,1)} %wg.1, f32[1]{0:T(128)S(6)} %copy.16.ld_ref, ...), custom_call_target="tpu_custom_call" | custom-call | tf_op jit(solution)/shard_map/retention/pallas_call | solution.py:378
  80.8 2.3 %copy.17 = bf16[4,64,2048]{2,1,0:T(8,128)(2,1)} copy(bf16[4,64,2048]{2,1,0:T(8,128)(2,1)} %retention.1) | data formatting | bytes 2097152

commit v2 on v1

v2 whole, which is shorter than its diff:
```python
import functools

import jax
import jax.numpy as jnp
import numpy as np
from jax import lax
from jax.experimental import pallas as pl
from jax.experimental.pallas import tpu as pltpu
from jax.sharding import PartitionSpec as P

MESH = pl.DeviceIdType.MESH
F32 = jnp.float32
BF16 = jnp.bfloat16
HD = 128
BLOCK = 128
NY = 4
RMS_EPS = 1e-06
GROUP_EPS = 1e-05
ROPE_BASE = 10000.0


def rotary_tables(blocks):
    half = HD // 2
    rate = ROPE_BASE ** (-np.arange(half, dtype=np.float64) / half)
    rate = np.concatenate([rate, rate])
    inside = np.arange(BLOCK, dtype=np.float64)[:, None] * rate
    starts = BLOCK * np.arange(blocks, dtype=np.float64)[:, None] * rate
    tables = (np.cos(inside), np.sin(inside), np.cos(starts), np.sin(starts))
    return [t.astype(np.float32) for t in tables]


def kernel(
    nz, ny, tok_hbm, gain_hbm, wq, wk, wv, wg, ld_ref, ng_hbm, ow, pg_hbm, tab_hbm, out_ref,
    raw, tok, w, oww, gain, pg, tabs, crow, ctab, stab, dmat, qsc, ksc, qs, acc, gs, smat, esend, ybuf, zsnd, zbuf,
    msnd, mbuf, gsend, gat, osc, lsem, xs, xr, ps, pr, wxs, wxr, wfs, wfr, cs, cr, ys, yr, zs, zr, ms, mr, as_, ar,
    ready_a, ready_b,
):
    nseq, rows, width = raw.shape
    ntp = 8
    nchip = ntp // 2
    blocks = 2
    span = blocks * BLOCK
    qr = HD // ny
    quarter = width // 4
    chunk = quarter // 4
    sp = lax.axis_index("sp")
    me = lax.axis_index("tp")
    z, y = sp // ny, sp % ny
    chip, core = me // 2, me % 2
    partner = chip * 2 + 1 - core
    half, dl = chip // 2, me % 4
    mine, theirs = chip % 2, 1 - chip % 2
    pair_same = (half * 2 + theirs) * 2 + core
    pair_other = (half * 2 + theirs) * 2 + 1 - core
    mate = (nchip - 1 - chip) * 2 + core

    def at(zz, yy):
        return (zz + nz) % nz * ny + (yy + ny) % ny

    barrier = pltpu.get_barrier_semaphore()
    near = [(at(z, y + k), me) for k in range(1, ny)] + [(at(z - 1, y), me), (at(z + 1, y), me), (sp, mate)]
    peers = [(sp, partner), (sp, pair_same), (sp, pair_other)] + near
    for dev in peers:
        pl.semaphore_signal(barrier, inc=1, device_id=dev, device_id_type=MESH)

    raw_loads = [pltpu.make_async_copy(tok_hbm.at[s], raw.at[s], lsem.at[s]) for s in range(nseq)]
    gain_load = pltpu.make_async_copy(gain_hbm, gain, lsem.at[4])
    tab_load = pltpu.make_async_copy(tab_hbm, tabs, lsem.at[5])
    ng_load = pltpu.make_async_copy(ng_hbm, crow.at[0, pl.ds(0, 1)], lsem.at[6])
    pg_load = pltpu.make_async_copy(pg_hbm, pg, lsem.at[7])
    w_load = pltpu.make_async_copy(w.at[0], w.at[0], lsem.at[8])
    ow_load = pltpu.make_async_copy(oww, oww, lsem.at[9])
    gain_load.start()
    for load in raw_loads:
        load.start()
    ng_load.start()
    for j, src in enumerate((wq, wk, wv, wg)):
        pltpu.make_async_copy(src, w.at[0, :, j * HD:(j + 1) * HD], lsem.at[8]).start()
    tab_load.start()
    pg_load.start()
    for d in range(4):
        first = half * 4 + d
        second = (nchip - 1 - first // 2) * 2 + d % 2
        for i, h in enumerate((first, second)):
            src = ow.at[pl.ds(pl.multiple_of(h * HD, HD), HD), :]
            pltpu.make_async_copy(src, oww.at[(2 * d + i) * HD:(2 * d + i + 1) * HD, :], lsem.at[9]).start()

    def remote(src, dst, send, recv, dev):
        return pltpu.make_async_remote_copy(
            src_ref=src, dst_ref=dst, send_sem=send, recv_sem=recv, device_id=dev, device_id_type=MESH
        )

    def part_of(s, d):
        return tok.at[s, pl.ds(pl.multiple_of(d * rows, rows), rows), :]

    def own_send(s):
        ref = part_of(s, dl)
        return remote(ref, ref, xs.at[0], xr.at[s], (sp, pair_same))

    def own_recv(s):
        ref = part_of(s, theirs * 2 + core)
        return remote(ref, ref, xs.at[0], xr.at[s], (sp, pair_same))

    def pass_send(s, i):
        ref = part_of(s, (mine, theirs)[i] * 2 + core)
        return remote(ref, ref, ps.at[0], pr.at[s, i], (sp, partner))

    def pass_recv(s, i):
        ref = part_of(s, (mine, theirs)[i] * 2 + 1 - core)
        return remote(ref, ref, ps.at[0], pr.at[s, i], (sp, partner))

    my_quarter = (y % 2) * 2 + z % 2

    def w_rows(k, j):
        return w.at[k, pl.ds(pl.multiple_of(my_quarter * quarter + j * chunk, chunk), chunk), :]

    def w_send(j):
        return remote(w_rows(0, j), w_rows(1, j), wxs.at[0], wxr.at[j], (sp, mate))

    def w_recv(j):
        return remote(w_rows(1, j), w_rows(1, j), wxs.at[0], wxr.at[j], (sp, mate))

    def w_forward(j):
        w_recv(j).wait_recv()
        yy, zz = y + (1, 1, -1, -1)[j], z + (1, -1, 1, -1)[j]
        for dev in (at(z, yy), at(zz, y), at(zz, yy)):
            remote(w_rows(1, j), w_rows(1, j), wfs.at[0], wfr.at[0], (dev, me)).start()

    def w_rest(rows_):
        ref = w.at[1, 0:rows_, :]
        return remote(ref, ref, wfs.at[0], wfr.at[0], (sp, partner))

    def c_send():
        return remote(crow.at[0], crow.at[1], cs.at[0], cr.at[0], (sp, mate))

    def ycopy(s, k, to):
        src = esend.at[s, k, pl.ds(pl.multiple_of(to * qr, qr), qr), :]
        return remote(src, ybuf.at[s, y * 2 + half], ys.at[0], yr.at[s], (at(z, to), (me, mate)[k]))

    def zcopy(s, to):
        return remote(zsnd.at[s], zbuf.at[s, z], zs.at[to], zr.at[s, z], (to * ny + y, me))

    def zrecv(s, frm):
        ref = zbuf.at[s, frm]
        return remote(ref, ref, zs.at[frm], zr.at[s, frm], (frm * ny + y, me))

    def mcopy(s, k, to):
        src = msnd.at[s, to * 2 + (half, 1 - half)[k]]
        dst = mbuf.at[s, k, pl.ds(pl.multiple_of(y * qr, qr), qr), :]
        return remote(src, dst, ms.at[0], mr.at[s], (at(z, to), (me, mate)[k]))

    def acopy(s, to):
        src = gsend.at[s, pl.ds(pl.multiple_of(to * rows, rows), rows), :]
        dst = gat.at[s, :, pl.ds(pl.multiple_of(dl * 2 * HD, 2 * HD), 2 * HD)]
        return remote(src, dst, as_.at[0], ar.at[s], (sp, half * 4 + to))

    def whole(ref, send, recv):
        return remote(ref, ref, send, recv, (sp, partner))

    part = 16

    def norm_own(s):
        raw_loads[s].wait()

        @pl.loop(0, rows // part)
        def _(c):
            v = raw[s, pl.ds(pl.multiple_of(c * part, part), part), :].astype(F32)
            scale = lax.rsqrt(jnp.mean(v * v, axis=-1, keepdims=True) + RMS_EPS)
            at_ = pl.multiple_of(dl * rows + c * part, part)
            tok[s, pl.ds(at_, part), :] = (v * scale * gain[...]).astype(BF16)

    gain_load.wait()
    norm_own(0)
    ng_load.wait()
    crow[0, pl.ds(1, 7), :] = jnp.full((7, HD), ld_ref[0], F32)

    pl.semaphore_wait(barrier, len(peers))
    own_send(0).start()
    pass_send(0, 0).start()
    for dev in near:
        pl.semaphore_signal(ready_a, inc=1, device_id=dev, device_id_type=MESH)
    w_load.wait()
    for j in range(4):
        w_send(j).start()
    c_send().start()
    for s in range(1, nseq):
        norm_own(s)
        if s == 1:
            own_send(s).start()
        pass_send(s, 0).start()

    i_col = lax.broadcasted_iota(jnp.int32, (BLOCK, HD), 0).astype(F32)
    i_row = lax.broadcasted_iota(jnp.int32, (BLOCK, HD), 1).astype(F32)

    def decay(k, count):
        return jnp.exp(crow[k, pl.ds(1, 1), :] * count)

    def head_tables(k):
        ld = crow[k, pl.ds(1, 1), :]
        dist = i_col - i_row
        dmat[k] = jnp.where(dist >= 0, jnp.exp(ld * jnp.maximum(dist, 0.0)), 0.0)
        qsc[k] = jnp.exp(ld * (i_col + 1.0))
        ksc[k] = jnp.exp(ld * (BLOCK - 1.0 - i_col))

    head_tables(0)
    tab_load.wait()
    sign = jnp.where(i_row < HD // 2, -1.0, 1.0)
    for b in range(blocks):
        start = sp * nchip + half * blocks + b
        cb = tabs[2, pl.ds(start, 1), :]
        sb = tabs[3, pl.ds(start, 1), :]
        ctab[b] = tabs[0] * cb - tabs[1] * sb
        stab[b] = (tabs[1] * cb + tabs[0] * sb) * sign

    def rotate(u, b):
        return u * ctab[b] + pltpu.roll(u, HD // 2, 1) * stab[b]

    def work(s, k, b0, nb):
        proj = jnp.dot(
            tok[s, pl.ds(pl.multiple_of(b0 * BLOCK, BLOCK), nb * BLOCK), :], w[k], preferred_element_type=F32
        ).astype(BF16)
        for i in range(nb):
            b = b0 + i
            here = pl.ds(pl.multiple_of(b * BLOCK, BLOCK), BLOCK)
            p = proj[i * BLOCK:(i + 1) * BLOCK]
            q = rotate(p[:, :HD].astype(F32), b).astype(BF16)
            kk = (rotate(p[:, HD:2 * HD].astype(F32), b) * HD ** -0.5).astype(BF16)
            v = p[:, 2 * HD:3 * HD]
            g = p[:, 3 * HD:].astype(F32)
            scores = lax.dot_general(q, kk, (((1,), (1,)), ((), ())), preferred_element_type=F32)
            weights = (scores * dmat[k]).astype(BF16)
            acc[s, k, here, :] = jnp.dot(weights, v, preferred_element_type=F32)
            qs[s, k, here, :] = (q.astype(F32) * qsc[k]).astype(BF16)
            ks = (kk.astype(F32) * ksc[k]).astype(BF16)
            smat[s, k, b] = lax.dot_general(ks, v, (((0,), (0,)), ((), ())), preferred_element_type=F32)
            gs[s, k, here, :] = crow[k, pl.ds(0, 1), :] * (g * jax.nn.sigmoid(g))

    def state_out(s):
        for k in range(2):
            esend[s, k] = (smat[s, k, 0] * decay(k, float(BLOCK)) + smat[s, k, 1]).astype(BF16)
        ybuf[s, y * 2 + half] = esend[s, 0, pl.ds(pl.multiple_of(y * qr, qr), qr), :]
        for to in range(ny):
            ycopy(s, 1, (y + to) % ny).start()
            if to:
                ycopy(s, 0, (y + to) % ny).start()
        for k in range(2):
            here = pl.ds(BLOCK, BLOCK)
            acc[s, k, here, :] += jnp.dot(
                qs[s, k, here, :], smat[s, k, 0].astype(BF16), preferred_element_type=F32
            )

    def state_row(s):
        whole(ybuf.at[s, pl.ds(0, 2 * ny - 1)], ys.at[0], yr.at[s]).wait_recv()
        step = decay(0, float(span))
        total = ybuf[s, 0].astype(F32)
        for k in range(1, 2 * ny):
            total = total * step + ybuf[s, k].astype(F32)
        zsnd[s] = total.astype(BF16)

        @pl.loop(z + 1, nz)
        def _(to):
            zcopy(s, to).start()

    def state_back(s):
        step = decay(0, float(span))
        row_step = decay(0, float(span * 2 * ny))

        def add(frm, total):
            zrecv(s, frm).wait_recv()
            return total * row_step + zbuf[s, frm].astype(F32)

        carried = lax.fori_loop(0, z, add, jnp.zeros((qr, HD), F32))
        for k in range(2 * ny):
            msnd[s, k] = carried.astype(BF16)
            if k < 2 * ny - 1:
                carried = carried * step + ybuf[s, k].astype(F32)
        mbuf[s, 0, pl.ds(pl.multiple_of(y * qr, qr), qr), :] = msnd[s, y * 2 + half]
        for to in range(ny):
            mcopy(s, 1, (y + to) % ny).start()
            if to:
                mcopy(s, 0, (y + to) % ny).start()

    def read_out(s):
        whole(ybuf.at[s, pl.ds(0, 2 * ny - 1)], ms.at[0], mr.at[s]).wait_recv()
        for k in range(2):
            memory = mbuf[s, k]
            for b in range(blocks):
                here = pl.ds(b * BLOCK, BLOCK)
                kept = jnp.dot(qs[s, k, here, :], memory, preferred_element_type=F32)
                kept = acc[s, k, here, :] + kept * decay(k, float(BLOCK * b))
                kept = kept - jnp.mean(kept, axis=-1, keepdims=True)
                spread = jnp.mean(kept * kept, axis=-1, keepdims=True)
                kept = kept * lax.rsqrt(spread + GROUP_EPS) * gs[s, k, here, :]
                gsend[s, here, k * HD:(k + 1) * HD] = kept.astype(BF16)
        for k in range(1, 4):
            acopy(s, (dl + k) % 4).start()
        own = gsend[s, pl.ds(pl.multiple_of(dl * rows, rows), rows), :]
        gat[s, :, pl.ds(pl.multiple_of(dl * 2 * HD, 2 * HD), 2 * HD)] = own

    def mix(s):
        whole(gat.at[s, :, 0:6 * HD], as_.at[0], ar.at[s]).wait_recv()
        osc[...] = jnp.dot(gat[s], oww[...], preferred_element_type=F32)

        @pl.loop(0, rows // part)
        def _(c):
            here = pl.ds(pl.multiple_of(c * part, part), part)
            v = osc[here, :]
            scale = lax.rsqrt(jnp.mean(v * v, axis=-1, keepdims=True) + RMS_EPS)
            out_ref[s, here, :] = (v * scale * pg[...]).astype(BF16)

    @pl.loop(0, nseq)
    def _(s):
        pass_recv(s, 0).wait_recv()
        work(s, 0, mine, 1)

    pl.semaphore_wait(ready_a, len(near))
    for dev in ((at(z - 2, y), me), (at(z + 2, y), me)):
        pl.semaphore_signal(ready_b, inc=1, device_id=dev, device_id_type=MESH)
    w_forward(0)
    for s in range(2):
        own_recv(s).wait_recv()
        pass_send(s, 1).start()
        own_send(s + 2).start()
        w_forward(1 + 2 * s)
        pass_recv(s, 1).wait_recv()
        work(s, 0, theirs, 1)
        if s == 0:
            w_forward(2)
    whole(crow.at[1], cs.at[0], cr.at[0]).wait_recv()
    head_tables(1)
    w_rest(3 * quarter).wait_recv()

    @pl.loop(0, 2)
    def _(s):
        work(s, 1, 0, 2)
        state_out(s)

    own_recv(2).wait_recv()
    pass_send(2, 1).start()
    pass_recv(2, 1).wait_recv()
    work(2, 0, theirs, 1)
    work(2, 1, 0, 2)
    state_out(2)
    work(3, 1, mine, 1)
    pl.semaphore_wait(ready_b, 2)
    state_row(0)
    state_row(1)
    own_recv(3).wait_recv()
    pass_send(3, 1).start()
    pass_recv(3, 1).wait_recv()
    work(3, 0, theirs, 1)
    work(3, 1, theirs, 1)
    state_out(3)
    state_row(2)
    state_row(3)
    state_back(0)
    state_back(1)
    state_back(2)
    read_out(0)
    read_out(1)
    state_back(3)
    ow_load.wait()
    pg_load.wait()
    read_out(2)
    mix(0)
    mix(1)
    read_out(3)
    mix(2)
    mix(3)

    whole(raw, xs.at[0], xr.at[0]).wait_send()
    whole(tok.at[:, 0:2 * rows, :], ps.at[0], pr.at[0, 0]).wait_send()
    whole(w.at[1, 0:quarter, :], wxs.at[0], wxr.at[0]).wait_send()
    w_rest(3 * quarter).wait_send()
    whole(crow.at[0], cs.at[0], cr.at[0]).wait_send()
    whole(ybuf.at[:, pl.ds(0, 2 * ny - 1)], ys.at[0], yr.at[0]).wait_send()
    whole(ybuf.at[:, pl.ds(0, 2 * ny - 1)], ms.at[0], mr.at[0]).wait_send()
    whole(gat.at[:, :, 0:6 * HD], as_.at[0], ar.at[0]).wait_send()

    @pl.loop(z + 1, nz)
    def _(to):
        whole(zsnd, zs.at[to], zr.at[0, to]).wait_send()


def body(nz, ny, tokens, in_gain, wq, wk, wv, wg, log_decay, norm_gain, out_weight, post_gain):
    nseq, rows, width = tokens.shape
    ntp = 8
    stretch = rows * ntp
    half = stretch // 2
    tables = jnp.asarray(np.stack(rotary_tables(BLOCK)))
    qr = HD // ny
    vmem, hbm, smem = (pl.BlockSpec(memory_space=m) for m in (pltpu.VMEM, pl.ANY, pltpu.SMEM))
    dma = pltpu.SemaphoreType.DMA
    signal = pltpu.SemaphoreType.REGULAR
    scratch = [
        pltpu.VMEM((nseq, rows, width), BF16),
        pltpu.VMEM((nseq, half, width), BF16),
        pltpu.VMEM((2, width, 4 * HD), BF16),
        pltpu.VMEM(out_weight.shape, BF16),
        pltpu.VMEM((1, width), F32),
        pltpu.VMEM((1, width), F32),
        pltpu.VMEM(tables.shape, F32),
        pltpu.VMEM((2, 8, HD), F32),
        pltpu.VMEM((2, BLOCK, HD), F32),
        pltpu.VMEM((2, BLOCK, HD), F32),
        pltpu.VMEM((2, BLOCK, HD), F32),
        pltpu.VMEM((2, BLOCK, HD), F32),
        pltpu.VMEM((2, BLOCK, HD), F32),
        pltpu.VMEM((nseq, 2, half, HD), BF16),
        pltpu.VMEM((nseq, 2, half, HD), F32),
        pltpu.VMEM((nseq, 2, half, HD), F32),
        pltpu.VMEM((nseq, 2, 2, HD, HD), F32),
        pltpu.VMEM((nseq, 2, HD, HD), BF16),
        pltpu.VMEM((nseq, 2 * ny, qr, HD), BF16),
        pltpu.VMEM((nseq, qr, HD), BF16),
        pltpu.VMEM((nseq, nz, qr, HD), BF16),
        pltpu.VMEM((nseq, 2 * ny, qr, HD), BF16),
        pltpu.VMEM((nseq, 2, HD, HD), BF16),
        pltpu.VMEM((nseq, half, 2 * HD), BF16),
        pltpu.VMEM((nseq, rows, ntp * HD), BF16),
        pltpu.VMEM((rows, width), F32),
        dma((10,)),
        dma((1,)), dma((nseq,)), dma((1,)), dma((nseq, 2)), dma((1,)), dma((4,)), dma((1,)), dma((1,)),
        dma((1,)), dma((1,)), dma((1,)), dma((nseq,)), dma((nz,)), dma((nseq, nz)), dma((1,)), dma((nseq,)),
        dma((1,)), dma((nseq,)), signal, signal,
    ]
    return pl.pallas_call(
        functools.partial(kernel, nz, ny),
        out_shape=jax.ShapeDtypeStruct(tokens.shape, BF16),
        in_specs=[hbm] * 6 + [smem] + [hbm] * 4,
        out_specs=vmem,
        scratch_shapes=scratch,
        name="retention",
        compiler_params=pltpu.CompilerParams(
            collective_id=0, has_side_effects=True, vmem_limit_bytes=60 * 1024 * 1024
        ),
    )(
        tokens, in_gain.reshape(1, -1), wq, wk, wv, wg, log_decay, norm_gain.reshape(1, -1), out_weight,
        post_gain.reshape(1, -1), tables,
    )


def solution(mesh):
    both = ("sp", "tp")
    nz = mesh.shape["sp"] // NY
    return jax.shard_map(
        functools.partial(body, nz, NY),
        mesh=mesh,
        in_specs=(
            P(None, both, None), P(), P(None, "tp"), P(None, "tp"), P(None, "tp"), P(None, "tp"), P("tp"), P("tp"),
            P(), P(),
        ),
        out_specs=P(None, both, None),
        check_vma=False,
    )
```

time: 83.2 us -> 68.5 us (0.82)
  Pallas kernels: 80.1 us -> 65.4 us
    pallas_call x1, Pallas kernels: 80.1 us -> 65.4 us  [body(): pl.pallas_call(functools.partial(kernel, nz, ny), out_shape=jax.ShapeDtyp...]
where the time goes in v2:
time: 68.5 us; the launch traced here: 68.4 us
  Pallas kernels  65.4 us (95%)
  local copies, waits for them, and re-layouts  2.3 us (3%)
    pallas_call x1, Pallas kernels, body(): pl.pallas_call(functools.partial(kernel, nz, ny), out_shape=jax.ShapeDtyp...  65.4 us
    unnamed x1, local copies, waits for them, and re-layouts  2.3 us

profile of v2, /device:TPU:1, one launch (start us, length us, event | category | flops | bytes accessed | tf_op | source)
XLA Modules:
  0.0 68.4 jit_solution(9284719543402326162)
XLA Ops:
  0.7 65.4 %retention.1 = bf16[4,64,2048]{2,1,0:T(8,128)(2,1)} custom-call(bf16[4,64,2048]{2,1,0:T(8,128)(2,1)} %tok_hbm.1, f32[1,2048]{1,0:T(1,128)} %bitcast.3, bf16[2048,128]{1,0:T(8,128)(2,1)} %wq.1, bf16[2048,128]{1,0:T(8,128)(2,1)} %wk.1, bf16[2048,128]{1,0:T(8,128)(2,1)} %wv.1, bf16[2048,128]{1,0:T(8,128)(2,1)} %wg.1, f32[1]{0:T(128)S(6)} %copy.13.ld_ref, ...), custom_call_target="tpu_custom_call" | custom-call | tf_op jit(solution)/shard_map/retention/pallas_call | solution.py:427
  66.1 2.3 %copy.14 = bf16[4,64,2048]{2,1,0:T(8,128)(2,1)} copy(bf16[4,64,2048]{2,1,0:T(8,128)(2,1)} %retention.1) | data formatting | bytes 2097152

commit v3 on v2

--- a/solution.py
+++ b/solution.py
@@ -31,8 +31,8 @@
 
 def kernel(
     nz, ny, tok_hbm, gain_hbm, wq, wk, wv, wg, ld_ref, ng_hbm, ow, pg_hbm, tab_hbm, out_ref,
-    raw, tok, w, oww, gain, pg, tabs, crow, ctab, stab, dmat, qsc, ksc, qs, acc, gs, smat, esend, ybuf, zsnd, zbuf,
-    msnd, mbuf, gsend, gat, osc, lsem, xs, xr, ps, pr, wxs, wxr, wfs, wfr, cs, cr, ys, yr, zs, zr, ms, mr, as_, ar,
+    raw, tok, w, oww, gain, pg, tabs, crow, ctab, stab, dmat, qsc, ksc, kbuf, vbuf, qs, acc, gs, smat, esend, ybuf,
+    zsnd, zbuf, msnd, mbuf, gsend, gat, osc, lsem, xs, xr, ps, pr, wxs, wxr, wfs, wfr, cs, cr, ys, yr, zs, zr, ms, mr, as_, ar,
     ready_a, ready_b,
 ):
     nseq, rows, width = raw.shape
@@ -68,14 +68,15 @@
     tab_load = pltpu.make_async_copy(tab_hbm, tabs, lsem.at[5])
     ng_load = pltpu.make_async_copy(ng_hbm, crow.at[0, pl.ds(0, 1)], lsem.at[6])
     pg_load = pltpu.make_async_copy(pg_hbm, pg, lsem.at[7])
-    w_load = pltpu.make_async_copy(w.at[0], w.at[0], lsem.at[8])
-    ow_load = pltpu.make_async_copy(oww, oww, lsem.at[9])
+    w_loads = [pltpu.make_async_copy(w.at[0, c], w.at[0, c], lsem.at[8 + c]) for c in range(2)]
+    ow_load = pltpu.make_async_copy(oww, oww, lsem.at[10])
     gain_load.start()
     for load in raw_loads:
         load.start()
     ng_load.start()
-    for j, src in enumerate((wq, wk, wv, wg)):
-        pltpu.make_async_copy(src, w.at[0, :, j * HD:(j + 1) * HD], lsem.at[8]).start()
+    for j, src in enumerate((wk, wv, wq, wg)):
+        cols = j % 2 * HD
+        pltpu.make_async_copy(src, w.at[0, j // 2, :, cols:cols + HD], lsem.at[8 + j // 2]).start()
     tab_load.start()
     pg_load.start()
     for d in range(4):
@@ -83,7 +84,7 @@
         second = (nchip - 1 - first // 2) * 2 + d % 2
         for i, h in enumerate((first, second)):
             src = ow.at[pl.ds(pl.multiple_of(h * HD, HD), HD), :]
-            pltpu.make_async_copy(src, oww.at[(2 * d + i) * HD:(2 * d + i + 1) * HD, :], lsem.at[9]).start()
+            pltpu.make_async_copy(src, oww.at[(2 * d + i) * HD:(2 * d + i + 1) * HD, :], lsem.at[10]).start()
 
     def remote(src, dst, send, recv, dev):
         return pltpu.make_async_remote_copy(
@@ -112,7 +113,8 @@
     my_quarter = (y % 2) * 2 + z % 2
 
     def w_rows(k, j):
-        return w.at[k, pl.ds(pl.multiple_of(my_quarter * quarter + j * chunk, chunk), chunk), :]
+        at_ = pl.multiple_of(my_quarter * quarter + j % 4 * chunk, chunk)
+        return w.at[k, j // 4, pl.ds(at_, chunk), :]
 
     def w_send(j):
         return remote(w_rows(0, j), w_rows(1, j), wxs.at[0], wxr.at[j], (sp, mate))
@@ -122,13 +124,13 @@
 
     def w_forward(j):
         w_recv(j).wait_recv()
-        yy, zz = y + (1, 1, -1, -1)[j], z + (1, -1, 1, -1)[j]
-        for dev in (at(z, yy), at(zz, y), at(zz, yy)):
-            remote(w_rows(1, j), w_rows(1, j), wfs.at[0], wfr.at[0], (dev, me)).start()
-
-    def w_rest(rows_):
-        ref = w.at[1, 0:rows_, :]
-        return remote(ref, ref, wfs.at[0], wfr.at[0], (sp, partner))
+        yy, zz = y + (1, -1)[j % 2], z + (1, -1)[j // 2 % 2]
+        for dev in (at(zz, yy), at(z, yy), at(zz, y)):
+            remote(w_rows(1, j), w_rows(1, j), wfs.at[0], wfr.at[j // 4], (dev, me)).start()
+
+    def w_rest(c):
+        ref = w.at[1, c, 0:3 * quarter, :]
+        return remote(ref, ref, wfs.at[0], wfr.at[c], (sp, partner))
 
     def c_send():
         return remote(crow.at[0], crow.at[1], cs.at[0], cr.at[0], (sp, mate))
@@ -179,9 +181,10 @@
     pass_send(0, 0).start()
     for dev in near:
         pl.semaphore_signal(ready_a, inc=1, device_id=dev, device_id_type=MESH)
-    w_load.wait()
-    for j in range(4):
-        w_send(j).start()
+    for c in range(2):
+        w_loads[c].wait()
+        for j in range(4 * c, 4 * c + 4):
+            w_send(j).start()
     c_send().start()
     for s in range(1, nseq):
         norm_own(s)
@@ -215,24 +218,37 @@
     def rotate(u, b):
         return u * ctab[b] + pltpu.roll(u, HD // 2, 1) * stab[b]
 
-    def work(s, k, b0, nb):
-        proj = jnp.dot(
-            tok[s, pl.ds(pl.multiple_of(b0 * BLOCK, BLOCK), nb * BLOCK), :], w[k], preferred_element_type=F32
-        ).astype(BF16)
+    def tokens_of(s, b0, nb):
+        return tok[s, pl.ds(pl.multiple_of(b0 * BLOCK, BLOCK), nb * BLOCK), :]
+
+    def block_at(b):
+        return pl.ds(pl.multiple_of(b * BLOCK, BLOCK), BLOCK)
+
+    def keys(s, k, b0, nb):
+        proj = jnp.dot(tokens_of(s, b0, nb), w[k, 0], preferred_element_type=F32).astype(BF16)
         for i in range(nb):
             b = b0 + i
-            here = pl.ds(pl.multiple_of(b * BLOCK, BLOCK), BLOCK)
+            here = block_at(b)
+            p = proj[i * BLOCK:(i + 1) * BLOCK]
+            kk = (rotate(p[:, :HD].astype(F32), b) * HD ** -0.5).astype(BF16)
+            v = p[:, HD:]
+            kbuf[s, k, here, :] = kk
+            vbuf[s, k, here, :] = v
+            ks = (kk.astype(F32) * ksc[k]).astype(BF16)
+            smat[s, k, b] = lax.dot_general(ks, v, (((0,), (0,)), ((), ())), preferred_element_type=F32)
+
+    def queries(s, k, b0, nb):
+        proj = jnp.dot(tokens_of(s, b0, nb), w[k, 1], preferred_element_type=F32).astype(BF16)
+        for i in range(nb):
+            b = b0 + i
+            here = block_at(b)
             p = proj[i * BLOCK:(i + 1) * BLOCK]
             q = rotate(p[:, :HD].astype(F32), b).astype(BF16)
-            kk = (rotate(p[:, HD:2 * HD].astype(F32), b) * HD ** -0.5).astype(BF16)
-            v = p[:, 2 * HD:3 * HD]
-            g = p[:, 3 * HD:].astype(F32)
-            scores = lax.dot_general(q, kk, (((1,), (1,)), ((), ())), preferred_element_type=F32)
+            g = p[:, HD:].astype(F32)
+            scores = lax.dot_general(q, kbuf[s, k, here, :], (((1,), (1,)), ((), ())), preferred_element_type=F32)
             weights = (scores * dmat[k]).astype(BF16)
-            acc[s, k, here, :] = jnp.dot(weights, v, preferred_element_type=F32)
+            acc[s, k, here, :] = jnp.dot(weights, vbuf[s, k, here, :], preferred_element_type=F32)
             qs[s, k, here, :] = (q.astype(F32) * qsc[k]).astype(BF16)
-            ks = (kk.astype(F32) * ksc[k]).astype(BF16)
-            smat[s, k, b] = lax.dot_general(ks, v, (((0,), (0,)), ((), ())), preferred_element_type=F32)
             gs[s, k, here, :] = crow[k, pl.ds(0, 1), :] * (g * jax.nn.sigmoid(g))
 
     def state_out(s):
@@ -243,11 +259,6 @@
             ycopy(s, 1, (y + to) % ny).start()
             if to:
                 ycopy(s, 0, (y + to) % ny).start()
-        for k in range(2):
-            here = pl.ds(BLOCK, BLOCK)
-            acc[s, k, here, :] += jnp.dot(
-                qs[s, k, here, :], smat[s, k, 0].astype(BF16), preferred_element_type=F32
-            )
 
     def state_row(s):
         whole(ybuf.at[s, pl.ds(0, 2 * ny - 1)], ys.at[0], yr.at[s]).wait_recv()
@@ -286,8 +297,9 @@
             memory = mbuf[s, k]
             for b in range(blocks):
                 here = pl.ds(b * BLOCK, BLOCK)
-                kept = jnp.dot(qs[s, k, here, :], memory, preferred_element_type=F32)
-                kept = acc[s, k, here, :] + kept * decay(k, float(BLOCK * b))
+                if b:
+                    memory = (smat[s, k, 0] + memory.astype(F32) * decay(k, float(BLOCK))).astype(BF16)
+                kept = acc[s, k, here, :] + jnp.dot(qs[s, k, here, :], memory, preferred_element_type=F32)
                 kept = kept - jnp.mean(kept, axis=-1, keepdims=True)
                 spread = jnp.mean(kept * kept, axis=-1, keepdims=True)
                 kept = kept * lax.rsqrt(spread + GROUP_EPS) * gs[s, k, here, :]
@@ -311,50 +323,67 @@
     @pl.loop(0, nseq)
     def _(s):
         pass_recv(s, 0).wait_recv()
-        work(s, 0, mine, 1)
+        keys(s, 0, mine, 1)
+        queries(s, 0, mine, 1)
 
     pl.semaphore_wait(ready_a, len(near))
     for dev in ((at(z - 2, y), me), (at(z + 2, y), me)):
         pl.semaphore_signal(ready_b, inc=1, device_id=dev, device_id_type=MESH)
-    w_forward(0)
-    for s in range(2):
+
+    def take_pair(s):
         own_recv(s).wait_recv()
         pass_send(s, 1).start()
-        own_send(s + 2).start()
-        w_forward(1 + 2 * s)
-        pass_recv(s, 1).wait_recv()
-        work(s, 0, theirs, 1)
-        if s == 0:
-            w_forward(2)
+        if s + 2 < nseq:
+            own_send(s + 2).start()
+
+    for j in range(3):
+        w_forward(j)
+    take_pair(0)
+    w_forward(3)
+    pass_recv(0, 1).wait_recv()
+    keys(0, 0, theirs, 1)
+    w_forward(4)
+    queries(0, 0, theirs, 1)
+    w_forward(5)
     whole(crow.at[1], cs.at[0], cr.at[0]).wait_recv()
     head_tables(1)
-    w_rest(3 * quarter).wait_recv()
-
-    @pl.loop(0, 2)
-    def _(s):
-        work(s, 1, 0, 2)
-        state_out(s)
-
-    own_recv(2).wait_recv()
-    pass_send(2, 1).start()
+    w_rest(0).wait_recv()
+    w_forward(6)
+    keys(0, 1, 0, 2)
+    state_out(0)
+    take_pair(1)
+    w_forward(7)
+    pass_recv(1, 1).wait_recv()
+    keys(1, 0, theirs, 1)
+    keys(1, 1, 0, 2)
+    state_out(1)
+    keys(2, 1, mine, 1)
+    keys(3, 1, mine, 1)
+    queries(1, 0, theirs, 1)
+    take_pair(2)
+    w_rest(1).wait_recv()
+    queries(0, 1, 0, 2)
     pass_recv(2, 1).wait_recv()
-    work(2, 0, theirs, 1)
-    work(2, 1, 0, 2)
+    keys(2, 0, theirs, 1)
+    keys(2, 1, theirs, 1)
     state_out(2)
-    work(3, 1, mine, 1)
     pl.semaphore_wait(ready_b, 2)
     state_row(0)
     state_row(1)
-    own_recv(3).wait_recv()
-    pass_send(3, 1).start()
+    queries(1, 1, 0, 2)
+    take_pair(3)
+    queries(2, 0, theirs, 1)
     pass_recv(3, 1).wait_recv()
-    work(3, 0, theirs, 1)
-    work(3, 1, theirs, 1)
+    keys(3, 0, theirs, 1)
+    keys(3, 1, theirs, 1)
     state_out(3)
     state_row(2)
-    state_row(3)
+    queries(2, 1, 0, 2)
     state_back(0)
     state_back(1)
+    queries(3, 0, theirs, 1)
+    queries(3, 1, 0, 2)
+    state_row(3)
     state_back(2)
     read_out(0)
     read_out(1)
@@ -370,8 +399,8 @@
 
     whole(raw, xs.at[0], xr.at[0]).wait_send()
     whole(tok.at[:, 0:2 * rows, :], ps.at[0], pr.at[0, 0]).wait_send()
-    whole(w.at[1, 0:quarter, :], wxs.at[0], wxr.at[0]).wait_send()
-    w_rest(3 * quarter).wait_send()
+    whole(w.at[1, :, 0:quarter, :], wxs.at[0], wxr.at[0]).wait_send()
+    whole(w.at[1, :, 0:3 * quarter, :], wfs.at[0], wfr.at[0]).wait_send()
     whole(crow.at[0], cs.at[0], cr.at[0]).wait_send()
     whole(ybuf.at[:, pl.ds(0, 2 * ny - 1)], ys.at[0], yr.at[0]).wait_send()
     whole(ybuf.at[:, pl.ds(0, 2 * ny - 1)], ms.at[0], mr.at[0]).wait_send()
@@ -395,7 +424,7 @@
     scratch = [
         pltpu.VMEM((nseq, rows, width), BF16),
         pltpu.VMEM((nseq, half, width), BF16),
-        pltpu.VMEM((2, width, 4 * HD), BF16),
+        pltpu.VMEM((2, 2, width, 2 * HD), BF16),
         pltpu.VMEM(out_weight.shape, BF16),
         pltpu.VMEM((1, width), F32),
         pltpu.VMEM((1, width), F32),
@@ -406,6 +435,8 @@
         pltpu.VMEM((2, BLOCK, HD), F32),
         pltpu.VMEM((2, BLOCK, HD), F32),
         pltpu.VMEM((2, BLOCK, HD), F32),
+        pltpu.VMEM((nseq, 2, half, HD), BF16),
+        pltpu.VMEM((nseq, 2, half, HD), BF16),
         pltpu.VMEM((nseq, 2, half, HD), BF16),
         pltpu.VMEM((nseq, 2, half, HD), F32),
         pltpu.VMEM((nseq, 2, half, HD), F32),
@@ -419,8 +450,8 @@
         pltpu.VMEM((nseq, half, 2 * HD), BF16),
         pltpu.VMEM((nseq, rows, ntp * HD), BF16),
         pltpu.VMEM((rows, width), F32),
-        dma((10,)),
-        dma((1,)), dma((nseq,)), dma((1,)), dma((nseq, 2)), dma((1,)), dma((4,)), dma((1,)), dma((1,)),
+        dma((11,)),
+        dma((1,)), dma((nseq,)), dma((1,)), dma((nseq, 2)), dma((1,)), dma((8,)), dma((1,)), dma((2,)),
         dma((1,)), dma((1,)), dma((1,)), dma((nseq,)), dma((nz,)), dma((nseq, nz)), dma((1,)), dma((nseq,)),
         dma((1,)), dma((nseq,)), signal, signal,
     ]

time: 68.5 us -> 60.5 us (0.88)
  Pallas kernels: 65.4 us -> 57.4 us
    pallas_call x1, Pallas kernels: 65.4 us -> 57.4 us  [body(): pl.pallas_call(functools.partial(kernel, nz, ny), out_shape=jax.ShapeDtyp...]
where the time goes in v3:
time: 60.5 us; the launch traced here: 60.3 us
  Pallas kernels  57.4 us (95%)
  local copies, waits for them, and re-layouts  2.3 us (4%)
  between operations  0.66 us (1%)
    pallas_call x1, Pallas kernels, body(): pl.pallas_call(functools.partial(kernel, nz, ny), out_shape=jax.ShapeDtyp...  57.4 us
    unnamed x1, local copies, waits for them, and re-layouts  2.3 us

profile of v3, /device:TPU:1, one launch (start us, length us, event | category | flops | bytes accessed | tf_op | source)
XLA Modules:
  0.0 60.3 jit_solution(4615532493300178958)
XLA Ops:
  0.7 57.4 %retention.1 = bf16[4,64,2048]{2,1,0:T(8,128)(2,1)} custom-call(bf16[4,64,2048]{2,1,0:T(8,128)(2,1)} %tok_hbm.1, f32[1,2048]{1,0:T(1,128)} %bitcast.3, bf16[2048,128]{1,0:T(8,128)(2,1)} %wq.1, bf16[2048,128]{1,0:T(8,128)(2,1)} %wk.1, bf16[2048,128]{1,0:T(8,128)(2,1)} %wv.1, bf16[2048,128]{1,0:T(8,128)(2,1)} %wg.1, f32[1]{0:T(128)S(6)} %copy.13.ld_ref, ...), custom_call_target="tpu_custom_call" | custom-call | tf_op jit(solution)/shard_map/retention/pallas_call | solution.py:458
  58.0 2.3 %copy.14 = bf16[4,64,2048]{2,1,0:T(8,128)(2,1)} copy(bf16[4,64,2048]{2,1,0:T(8,128)(2,1)} %retention.1) | data formatting | bytes 2097152

commit v4 on v3

--- a/solution.py
+++ b/solution.py
@@ -29,10 +29,17 @@
     return [t.astype(np.float32) for t in tables]
 
 
+def row_scale(read, width):
+    total = jnp.square(read(0))
+    for c in range(1, width // HD):
+        total += jnp.square(read(c))
+    return lax.rsqrt(jnp.sum(total, axis=-1, keepdims=True) * (1.0 / width) + RMS_EPS)
+
+
 def kernel(
-    nz, ny, tok_hbm, gain_hbm, wq, wk, wv, wg, ld_ref, ng_hbm, ow, pg_hbm, tab_hbm, out_ref,
-    raw, tok, w, oww, gain, pg, tabs, crow, ctab, stab, dmat, qsc, ksc, kbuf, vbuf, qs, acc, gs, smat, esend, ybuf,
-    zsnd, zbuf, msnd, mbuf, gsend, gat, osc, lsem, xs, xr, ps, pr, wxs, wxr, wfs, wfr, cs, cr, ys, yr, zs, zr, ms, mr, as_, ar,
+    nz, ny, tok_hbm, gain_hbm, wq, wk, wv, wg, ld_ref, ng_hbm, ow, tab_hbm, gat, oww,
+    raw, tok, w, gain, tabs, crow, ctab, stab, dmat, qsc, ksc, kbuf, vbuf, qs, acc, gs, smat, esend, ybuf,
+    zsnd, zbuf, msnd, mbuf, gsend, lsem, xs, xr, ps, pr, wxs, wxr, wfs, wfr, cs, cr, ys, yr, zs, zr, ms, mr, as_, ar,
     ready_a, ready_b,
 ):
     nseq, rows, width = raw.shape
@@ -67,7 +74,6 @@
     gain_load = pltpu.make_async_copy(gain_hbm, gain, lsem.at[4])
     tab_load = pltpu.make_async_copy(tab_hbm, tabs, lsem.at[5])
     ng_load = pltpu.make_async_copy(ng_hbm, crow.at[0, pl.ds(0, 1)], lsem.at[6])
-    pg_load = pltpu.make_async_copy(pg_hbm, pg, lsem.at[7])
     w_loads = [pltpu.make_async_copy(w.at[0, c], w.at[0, c], lsem.at[8 + c]) for c in range(2)]
     ow_load = pltpu.make_async_copy(oww, oww, lsem.at[10])
     gain_load.start()
@@ -78,7 +84,6 @@
         cols = j % 2 * HD
         pltpu.make_async_copy(src, w.at[0, j // 2, :, cols:cols + HD], lsem.at[8 + j // 2]).start()
     tab_load.start()
-    pg_load.start()
     for d in range(4):
         first = half * 4 + d
         second = (nchip - 1 - first // 2) * 2 + d % 2
@@ -154,22 +159,19 @@
     def acopy(s, to):
         src = gsend.at[s, pl.ds(pl.multiple_of(to * rows, rows), rows), :]
         dst = gat.at[s, :, pl.ds(pl.multiple_of(dl * 2 * HD, 2 * HD), 2 * HD)]
-        return remote(src, dst, as_.at[0], ar.at[s], (sp, half * 4 + to))
+        return remote(src, dst, as_.at[0], ar.at[0], (sp, half * 4 + to))
 
     def whole(ref, send, recv):
         return remote(ref, ref, send, recv, (sp, partner))
 
-    part = 16
-
     def norm_own(s):
         raw_loads[s].wait()
-
-        @pl.loop(0, rows // part)
-        def _(c):
-            v = raw[s, pl.ds(pl.multiple_of(c * part, part), part), :].astype(F32)
-            scale = lax.rsqrt(jnp.mean(v * v, axis=-1, keepdims=True) + RMS_EPS)
-            at_ = pl.multiple_of(dl * rows + c * part, part)
-            tok[s, pl.ds(at_, part), :] = (v * scale * gain[...]).astype(BF16)
+        scale = row_scale(lambda c: raw[s, :, c * HD:(c + 1) * HD].astype(F32), width)
+        here = pl.ds(pl.multiple_of(dl * rows, rows), rows)
+        for c in range(width // HD):
+            cols = slice(c * HD, (c + 1) * HD)
+            v = raw[s, :, cols].astype(F32)
+            tok[s, here, cols] = (v * scale * gain[:, cols]).astype(BF16)
 
     gain_load.wait()
     norm_own(0)
@@ -181,11 +183,11 @@
     pass_send(0, 0).start()
     for dev in near:
         pl.semaphore_signal(ready_a, inc=1, device_id=dev, device_id_type=MESH)
+    c_send().start()
     for c in range(2):
         w_loads[c].wait()
         for j in range(4 * c, 4 * c + 4):
             w_send(j).start()
-    c_send().start()
     for s in range(1, nseq):
         norm_own(s)
         if s == 1:
@@ -309,17 +311,6 @@
         own = gsend[s, pl.ds(pl.multiple_of(dl * rows, rows), rows), :]
         gat[s, :, pl.ds(pl.multiple_of(dl * 2 * HD, 2 * HD), 2 * HD)] = own
 
-    def mix(s):
-        whole(gat.at[s, :, 0:6 * HD], as_.at[0], ar.at[s]).wait_recv()
-        osc[...] = jnp.dot(gat[s], oww[...], preferred_element_type=F32)
-
-        @pl.loop(0, rows // part)
-        def _(c):
-            here = pl.ds(pl.multiple_of(c * part, part), part)
-            v = osc[here, :]
-            scale = lax.rsqrt(jnp.mean(v * v, axis=-1, keepdims=True) + RMS_EPS)
-            out_ref[s, here, :] = (v * scale * pg[...]).astype(BF16)
-
     @pl.loop(0, nseq)
     def _(s):
         pass_recv(s, 0).wait_recv()
@@ -333,12 +324,13 @@
     def take_pair(s):
         own_recv(s).wait_recv()
         pass_send(s, 1).start()
-        if s + 2 < nseq:
-            own_send(s + 2).start()
-
-    for j in range(3):
-        w_forward(j)
+
+    w_forward(0)
+    own_send(2).start()
+    w_forward(1)
+    w_forward(2)
     take_pair(0)
+    own_send(3).start()
     w_forward(3)
     pass_recv(0, 1).wait_recv()
     keys(0, 0, theirs, 1)
@@ -361,8 +353,6 @@
     keys(3, 1, mine, 1)
     queries(1, 0, theirs, 1)
     take_pair(2)
-    w_rest(1).wait_recv()
-    queries(0, 1, 0, 2)
     pass_recv(2, 1).wait_recv()
     keys(2, 0, theirs, 1)
     keys(2, 1, theirs, 1)
@@ -370,32 +360,26 @@
     pl.semaphore_wait(ready_b, 2)
     state_row(0)
     state_row(1)
+    w_rest(1).wait_recv()
+    queries(0, 1, 0, 2)
+    take_pair(3)
     queries(1, 1, 0, 2)
-    take_pair(3)
-    queries(2, 0, theirs, 1)
     pass_recv(3, 1).wait_recv()
     keys(3, 0, theirs, 1)
     keys(3, 1, theirs, 1)
     state_out(3)
+    queries(2, 0, theirs, 1)
+    queries(2, 1, 0, 2)
     state_row(2)
-    queries(2, 1, 0, 2)
-    state_back(0)
-    state_back(1)
     queries(3, 0, theirs, 1)
     queries(3, 1, 0, 2)
     state_row(3)
-    state_back(2)
-    read_out(0)
-    read_out(1)
-    state_back(3)
+    for s in range(nseq):
+        state_back(s)
+    for s in range(nseq):
+        read_out(s)
     ow_load.wait()
-    pg_load.wait()
-    read_out(2)
-    mix(0)
-    mix(1)
-    read_out(3)
-    mix(2)
-    mix(3)
+    whole(gat.at[:, :, 0:6 * HD], as_.at[0], ar.at[0]).wait_recv()
 
     whole(raw, xs.at[0], xr.at[0]).wait_send()
     whole(tok.at[:, 0:2 * rows, :], ps.at[0], pr.at[0, 0]).wait_send()
@@ -411,6 +395,15 @@
         whole(zsnd, zs.at[to], zr.at[0, to]).wait_send()
 
 
+def mix_kernel(gat, oww, pg, out_ref, osc):
+    osc[...] = jnp.dot(gat[...], oww[...], preferred_element_type=F32)
+    width = osc.shape[1]
+    scale = row_scale(lambda c: osc[:, c * HD:(c + 1) * HD], width)
+    for c in range(width // HD):
+        cols = slice(c * HD, (c + 1) * HD)
+        out_ref[:, cols] = (osc[:, cols] * scale * pg[:, cols]).astype(BF16)
+
+
 def body(nz, ny, tokens, in_gain, wq, wk, wv, wg, log_decay, norm_gain, out_weight, post_gain):
     nseq, rows, width = tokens.shape
     ntp = 8
@@ -418,15 +411,13 @@
     half = stretch // 2
     tables = jnp.asarray(np.stack(rotary_tables(BLOCK)))
     qr = HD // ny
-    vmem, hbm, smem = (pl.BlockSpec(memory_space=m) for m in (pltpu.VMEM, pl.ANY, pltpu.SMEM))
+    vmem, hbm, smem = (pl.BlockSpec(memory_space=m) for m in (pltpu.VMEM, pltpu.HBM, pltpu.SMEM))
     dma = pltpu.SemaphoreType.DMA
     signal = pltpu.SemaphoreType.REGULAR
     scratch = [
         pltpu.VMEM((nseq, rows, width), BF16),
         pltpu.VMEM((nseq, half, width), BF16),
         pltpu.VMEM((2, 2, width, 2 * HD), BF16),
-        pltpu.VMEM(out_weight.shape, BF16),
-        pltpu.VMEM((1, width), F32),
         pltpu.VMEM((1, width), F32),
         pltpu.VMEM(tables.shape, F32),
         pltpu.VMEM((2, 8, HD), F32),
@@ -448,27 +439,41 @@
         pltpu.VMEM((nseq, 2 * ny, qr, HD), BF16),
         pltpu.VMEM((nseq, 2, HD, HD), BF16),
         pltpu.VMEM((nseq, half, 2 * HD), BF16),
-        pltpu.VMEM((nseq, rows, ntp * HD), BF16),
-        pltpu.VMEM((rows, width), F32),
         dma((11,)),
         dma((1,)), dma((nseq,)), dma((1,)), dma((nseq, 2)), dma((1,)), dma((8,)), dma((1,)), dma((2,)),
         dma((1,)), dma((1,)), dma((1,)), dma((nseq,)), dma((nz,)), dma((nseq, nz)), dma((1,)), dma((nseq,)),
-        dma((1,)), dma((nseq,)), signal, signal,
+        dma((1,)), dma((1,)), signal, signal,
     ]
-    return pl.pallas_call(
+    gathered, weight = pl.pallas_call(
         functools.partial(kernel, nz, ny),
-        out_shape=jax.ShapeDtypeStruct(tokens.shape, BF16),
-        in_specs=[hbm] * 6 + [smem] + [hbm] * 4,
-        out_specs=vmem,
+        out_shape=[pltpu.VMEM((nseq, rows, ntp * HD), BF16), pltpu.VMEM(out_weight.shape, BF16)],
+        in_specs=[hbm] * 6 + [smem] + [hbm] * 3,
+        out_specs=[vmem, vmem],
         scratch_shapes=scratch,
         name="retention",
         compiler_params=pltpu.CompilerParams(
-            collective_id=0, has_side_effects=True, vmem_limit_bytes=60 * 1024 * 1024
+            collective_id=0, has_side_effects=True, vmem_limit_bytes=62_300_000
         ),
     )(
-        tokens, in_gain.reshape(1, -1), wq, wk, wv, wg, log_decay, norm_gain.reshape(1, -1), out_weight,
-        post_gain.reshape(1, -1), tables,
+        tokens, in_gain.reshape(1, -1), wq, wk, wv, wg, log_decay, norm_gain.reshape(1, -1), out_weight, tables,
     )
+    every = nseq * rows
+    step = every // 2
+    mixed = pl.pallas_call(
+        mix_kernel,
+        out_shape=jax.ShapeDtypeStruct((every, width), BF16),
+        grid=(every // step,),
+        in_specs=[
+            pl.BlockSpec((step, ntp * HD), lambda i: (i, 0)),
+            pl.BlockSpec(out_weight.shape, lambda i: (0, 0)),
+            pl.BlockSpec((1, width), lambda i: (0, 0)),
+        ],
+        out_specs=pl.BlockSpec((step, width), lambda i: (i, 0)),
+        scratch_shapes=[pltpu.VMEM((step, width), F32)],
+        name="mix",
+        compiler_params=pltpu.CompilerParams(vmem_limit_bytes=16 * 1024 * 1024),
+    )(gathered.reshape(every, ntp * HD), weight, post_gain.reshape(1, -1))
+    return mixed.reshape(tokens.shape)
 
 
 def solution(mesh):

time: 60.5 us -> 55.4 us (0.916)
  Pallas kernels: 57.4 us -> 54.5 us
  local copies, waits for them, and re-layouts: 2.3 us -> 0.01 us
    pallas_call x1 -> x2, Pallas kernels: 57.4 us -> 54.5 us  [the longest x1 51.8 us: body(): pl.pallas_call(functools.partial(kernel, nz, ny), out_shape=[pltpu.VMEM((...]
    unnamed x1 -> x2, local copies, waits for them, and re-layouts: 2.3 us -> 0.01 us
where the time goes in v4:
time: 55.4 us; the launch traced here: 55.2 us
  Pallas kernels  54.5 us (98%)
  between operations  0.68 us (1%)
    pallas_call x1, Pallas kernels, body(): pl.pallas_call(functools.partial(kernel, nz, ny), out_shape=[pltpu.VMEM((...  51.8 us
    pallas_call x1, Pallas kernels, body(): pl.pallas_call(mix_kernel, out_shape=jax.ShapeDtypeStruct((every, width),...  2.65 us

profile of v4, /device:TPU:1, one launch (start us, length us, event | category | flops | bytes accessed | tf_op | source)
XLA Modules:
  0.0 55.2 jit_solution(8300840238626718928)
XLA Ops:
  0.0 0.0 copy-start
  0.7 51.8 %retention.1 = (bf16[4,64,1024]{2,1,0:T(8,128)(2,1)S(1)}, bf16[1024,2048]{1,0:T(8,128)(2,1)S(1)}) custom-call(bf16[4,64,2048]{2,1,0:T(8,128)(2,1)} %tok_hbm.1, f32[1,2048]{1,0:T(1,128)} %bitcast.7, bf16[2048,128]{1,0:T(8,128)(2,1)} %wq.1, bf16[2048,128]{1,0:T(8,128)(2,1)} %wk.1, bf16[2048,128]{1,0:T(8,128)(2,1)} %wv.1, bf16[2048,128]{1,0:T(8,128)(2,1)} %wg.1, ...), custom_call_target="tpu_custom_call" | custom-call | tf_op jit(solution)/shard_map/retention/pallas_call | solution.py:447
  52.5 0.0 copy-done
  52.5 2.6 %mix.1 = bf16[256,2048]{1,0:T(8,128)(2,1)} custom-call(bf16[256,1024]{1,0:T(8,128)(2,1)S(1)} %bitcast.5, bf16[1024,2048]{1,0:T(8,128)(2,1)S(1)} %get-tuple-element.8.oww, f32[1,2048]{1,0:T(1,128)S(1)} %bitcast.6), custom_call_target="tpu_custom_call" | custom-call | tf_op jit(solution)/shard_map/mix/pallas_call | solution.py:462
Async XLA Ops:
  0.0 52.5 %copy-start = (f32[2048]{0:T(1024)S(1)}, f32[2048]{0:T(1024)}, u32[]{:S(2)}) copy-start(f32[2048]{0:T(1024)} %param.20) | copy-start | bytes 24580

commit v5 on v4

--- a/solution.py
+++ b/solution.py
@@ -14,6 +14,7 @@
 HD = 128
 BLOCK = 128
 NY = 4
+VMEM_LIMIT = 62_000_000
 RMS_EPS = 1e-06
 GROUP_EPS = 1e-05
 ROPE_BASE = 10000.0
@@ -36,10 +37,19 @@
     return lax.rsqrt(jnp.sum(total, axis=-1, keepdims=True) * (1.0 / width) + RMS_EPS)
 
 
+def scale_rows(osc, pg, out, start, count):
+    width = osc.shape[1]
+    here = pl.ds(start, count)
+    scale = row_scale(lambda c: osc[here, c * HD:(c + 1) * HD], width)
+    for c in range(width // HD):
+        cols = slice(c * HD, (c + 1) * HD)
+        out[here, cols] = (osc[here, cols] * scale * pg[:, cols]).astype(BF16)
+
+
 def kernel(
-    nz, ny, tok_hbm, gain_hbm, wq, wk, wv, wg, ld_ref, ng_hbm, ow, tab_hbm, gat, oww,
-    raw, tok, w, gain, tabs, crow, ctab, stab, dmat, qsc, ksc, kbuf, vbuf, qs, acc, gs, smat, esend, ybuf,
-    zsnd, zbuf, msnd, mbuf, gsend, lsem, xs, xr, ps, pr, wxs, wxr, wfs, wfr, cs, cr, ys, yr, zs, zr, ms, mr, as_, ar,
+    nz, ny, tok_hbm, gain_hbm, wq, wk, wv, wg, ld_ref, ng_hbm, ow, pg_hbm, tab_hbm,
+    gat_late, oww, mixed, raw, tok, w, gain, pg, tabs, crow, ctab, stab, dmat, qsc, ksc, kbuf, vbuf, qs, acc, gs, smat, esend, ybuf,
+    zsnd, zbuf, msnd, mbuf, gsend, gat_early, osc, lsem, xs, xr, ps, pr, wxs, wxr, wfs, wfr, cs, cr, ys, yr, zs, zr, ms, mr, as_, ar,
     ready_a, ready_b,
 ):
     nseq, rows, width = raw.shape
@@ -60,30 +70,35 @@
     pair_same = (half * 2 + theirs) * 2 + core
     pair_other = (half * 2 + theirs) * 2 + 1 - core
     mate = (nchip - 1 - chip) * 2 + core
+    owners = (chip * 2 + 1, (nchip - 1 - chip) * 2 + 1)
 
     def at(zz, yy):
         return (zz + nz) % nz * ny + (yy + ny) % ny
 
     barrier = pltpu.get_barrier_semaphore()
     near = [(at(z, y + k), me) for k in range(1, ny)] + [(at(z - 1, y), me), (at(z + 1, y), me), (sp, mate)]
-    peers = [(sp, partner), (sp, pair_same), (sp, pair_other)] + near
+    near = near + [(sp, partner)]
+    peers = [(sp, pair_same), (sp, pair_other)] + near
     for dev in peers:
         pl.semaphore_signal(barrier, inc=1, device_id=dev, device_id_type=MESH)
 
     raw_loads = [pltpu.make_async_copy(tok_hbm.at[s], raw.at[s], lsem.at[s]) for s in range(nseq)]
     gain_load = pltpu.make_async_copy(gain_hbm, gain, lsem.at[4])
     tab_load = pltpu.make_async_copy(tab_hbm, tabs, lsem.at[5])
+    pg_load = pltpu.make_async_copy(pg_hbm, pg, lsem.at[7])
     ng_load = pltpu.make_async_copy(ng_hbm, crow.at[0, pl.ds(0, 1)], lsem.at[6])
     w_loads = [pltpu.make_async_copy(w.at[0, c], w.at[0, c], lsem.at[8 + c]) for c in range(2)]
     ow_load = pltpu.make_async_copy(oww, oww, lsem.at[10])
+    raw_loads[0].start()
     gain_load.start()
-    for load in raw_loads:
+    ng_load.start()
+    for load in raw_loads[1:]:
         load.start()
-    ng_load.start()
     for j, src in enumerate((wk, wv, wq, wg)):
         cols = j % 2 * HD
         pltpu.make_async_copy(src, w.at[0, j // 2, :, cols:cols + HD], lsem.at[8 + j // 2]).start()
     tab_load.start()
+    pg_load.start()
     for d in range(4):
         first = half * 4 + d
         second = (nchip - 1 - first // 2) * 2 + d % 2
@@ -137,12 +152,13 @@
         ref = w.at[1, c, 0:3 * quarter, :]
         return remote(ref, ref, wfs.at[0], wfr.at[c], (sp, partner))
 
-    def c_send():
-        return remote(crow.at[0], crow.at[1], cs.at[0], cr.at[0], (sp, mate))
+    def c_send(i):
+        return remote(crow.at[0], crow.at[1 + i], cs.at[0], cr.at[i], (sp, (mate, partner)[i]))
 
     def ycopy(s, k, to):
         src = esend.at[s, k, pl.ds(pl.multiple_of(to * qr, qr), qr), :]
-        return remote(src, ybuf.at[s, y * 2 + half], ys.at[0], yr.at[s], (at(z, to), (me, mate)[k]))
+        dst = ybuf.at[s, core * 2 * ny + y * 2 + half]
+        return remote(src, dst, ys.at[0], yr.at[s], (at(z, to), owners[k]))
 
     def zcopy(s, to):
         return remote(zsnd.at[s], zbuf.at[s, z], zs.at[to], zr.at[s, z], (to * ny + y, me))
@@ -151,15 +167,18 @@
         ref = zbuf.at[s, frm]
         return remote(ref, ref, zs.at[frm], zr.at[s, frm], (frm * ny + y, me))
 
-    def mcopy(s, k, to):
-        src = msnd.at[s, to * 2 + (half, 1 - half)[k]]
+    def mcopy(s, i, k, to):
+        src = msnd.at[s, i * 2 * ny + to * 2 + (half, 1 - half)[k]]
         dst = mbuf.at[s, k, pl.ds(pl.multiple_of(y * qr, qr), qr), :]
-        return remote(src, dst, ms.at[0], mr.at[s], (at(z, to), (me, mate)[k]))
+        return remote(src, dst, ms.at[0], mr.at[s], (at(z, to), owners[k] - 1 + i))
+
+    def gat_of(s):
+        return (gat_early, gat_late)[s // 2].at[pl.ds(s % 2 * rows, rows), :]
 
     def acopy(s, to):
         src = gsend.at[s, pl.ds(pl.multiple_of(to * rows, rows), rows), :]
-        dst = gat.at[s, :, pl.ds(pl.multiple_of(dl * 2 * HD, 2 * HD), 2 * HD)]
-        return remote(src, dst, as_.at[0], ar.at[0], (sp, half * 4 + to))
+        dst = gat_of(s).at[:, pl.ds(pl.multiple_of(dl * 2 * HD, 2 * HD), 2 * HD)]
+        return remote(src, dst, as_.at[0], ar.at[s // 2], (sp, half * 4 + to))
 
     def whole(ref, send, recv):
         return remote(ref, ref, send, recv, (sp, partner))
@@ -183,7 +202,8 @@
     pass_send(0, 0).start()
     for dev in near:
         pl.semaphore_signal(ready_a, inc=1, device_id=dev, device_id_type=MESH)
-    c_send().start()
+    c_send(0).start()
+    c_send(1).start()
     for c in range(2):
         w_loads[c].wait()
         for j in range(4 * c, 4 * c + 4):
@@ -253,48 +273,81 @@
             qs[s, k, here, :] = (q.astype(F32) * qsc[k]).astype(BF16)
             gs[s, k, here, :] = crow[k, pl.ds(0, 1), :] * (g * jax.nn.sigmoid(g))
 
+    far_first = [(1, ny // 2)]
+    for to in range(1, ny):
+        if to != ny // 2:
+            far_first.append((1, to))
+    far_first += [(0, ny // 2), (1, 0)]
+    for to in range(1, ny):
+        if to != ny // 2:
+            far_first.append((0, to))
+
     def state_out(s):
         for k in range(2):
             esend[s, k] = (smat[s, k, 0] * decay(k, float(BLOCK)) + smat[s, k, 1]).astype(BF16)
-        ybuf[s, y * 2 + half] = esend[s, 0, pl.ds(pl.multiple_of(y * qr, qr), qr), :]
-        for to in range(ny):
-            ycopy(s, 1, (y + to) % ny).start()
-            if to:
-                ycopy(s, 0, (y + to) % ny).start()
+        for k, to in far_first:
+            ycopy(s, k, (y + to) % ny).start()
+
+        @pl.when(core == 0)
+        def _():
+            ycopy(s, 0, y).start()
+
+        @pl.when(core == 1)
+        def _():
+            kept = esend[s, 0, pl.ds(pl.multiple_of(y * qr, qr), qr), :]
+            ybuf[s, 2 * ny + y * 2 + half] = kept
+
+    def owned_decay(i, count):
+        return decay((2, 0)[i], count)
 
     def state_row(s):
-        whole(ybuf.at[s, pl.ds(0, 2 * ny - 1)], ys.at[0], yr.at[s]).wait_recv()
-        step = decay(0, float(span))
-        total = ybuf[s, 0].astype(F32)
-        for k in range(1, 2 * ny):
-            total = total * step + ybuf[s, k].astype(F32)
-        zsnd[s] = total.astype(BF16)
-
-        @pl.loop(z + 1, nz)
-        def _(to):
-            zcopy(s, to).start()
+        @pl.when(core == 1)
+        def _():
+            whole(ybuf.at[s, pl.ds(0, 4 * ny - 1)], ys.at[0], yr.at[s]).wait_recv()
+            for i in range(2):
+                step = owned_decay(i, float(span))
+                total = ybuf[s, i * 2 * ny].astype(F32)
+                for k in range(1, 2 * ny):
+                    total = total * step + ybuf[s, i * 2 * ny + k].astype(F32)
+                zsnd[s, i] = total.astype(BF16)
+
+            @pl.loop(0, nz - 1 - z)
+            def _(k):
+                zcopy(s, nz - 1 - k).start()
 
     def state_back(s):
-        step = decay(0, float(span))
-        row_step = decay(0, float(span * 2 * ny))
-
-        def add(frm, total):
-            zrecv(s, frm).wait_recv()
-            return total * row_step + zbuf[s, frm].astype(F32)
-
-        carried = lax.fori_loop(0, z, add, jnp.zeros((qr, HD), F32))
-        for k in range(2 * ny):
-            msnd[s, k] = carried.astype(BF16)
-            if k < 2 * ny - 1:
-                carried = carried * step + ybuf[s, k].astype(F32)
-        mbuf[s, 0, pl.ds(pl.multiple_of(y * qr, qr), qr), :] = msnd[s, y * 2 + half]
-        for to in range(ny):
-            mcopy(s, 1, (y + to) % ny).start()
-            if to:
-                mcopy(s, 0, (y + to) % ny).start()
+        @pl.when(core == 1)
+        def _():
+            steps = [owned_decay(i, float(span)) for i in range(2)]
+            row_steps = [owned_decay(i, float(span * 2 * ny)) for i in range(2)]
+
+            def add(frm, totals):
+                zrecv(s, frm).wait_recv()
+                return tuple(totals[i] * row_steps[i] + zbuf[s, frm, i].astype(F32) for i in range(2))
+
+            zero = jnp.zeros((qr, HD), F32)
+            carried = lax.fori_loop(0, z, add, (zero, zero))
+            for i in range(2):
+                total = carried[i]
+                for k in range(2 * ny):
+                    msnd[s, i * 2 * ny + k] = total.astype(BF16)
+                    if k < 2 * ny - 1:
+                        total = total * steps[i] + ybuf[s, i * 2 * ny + k].astype(F32)
+            for k, to in far_first:
+                for i in range(2):
+                    mcopy(s, i, k, (y + to) % ny).start()
+            mcopy(s, 0, 0, y).start()
+            mbuf[s, 0, pl.ds(pl.multiple_of(y * qr, qr), qr), :] = msnd[s, 2 * ny + y * 2 + half]
 
     def read_out(s):
-        whole(ybuf.at[s, pl.ds(0, 2 * ny - 1)], ms.at[0], mr.at[s]).wait_recv()
+        @pl.when(core == 0)
+        def _():
+            whole(ybuf.at[s, pl.ds(0, 2 * ny)], ms.at[0], mr.at[s]).wait_recv()
+
+        @pl.when(core == 1)
+        def _():
+            whole(ybuf.at[s, pl.ds(0, 2 * ny - 1)], ms.at[0], mr.at[s]).wait_recv()
+
         for k in range(2):
             memory = mbuf[s, k]
             for b in range(blocks):
@@ -309,7 +362,7 @@
         for k in range(1, 4):
             acopy(s, (dl + k) % 4).start()
         own = gsend[s, pl.ds(pl.multiple_of(dl * rows, rows), rows), :]
-        gat[s, :, pl.ds(pl.multiple_of(dl * 2 * HD, 2 * HD), 2 * HD)] = own
+        gat_of(s)[:, pl.ds(pl.multiple_of(dl * 2 * HD, 2 * HD), 2 * HD)] = own
 
     @pl.loop(0, nseq)
     def _(s):
@@ -318,7 +371,8 @@
         queries(s, 0, mine, 1)
 
     pl.semaphore_wait(ready_a, len(near))
-    for dev in ((at(z - 2, y), me), (at(z + 2, y), me)):
+    far = ((at(z - 2, y), me), (at(z + 2, y), me), (sp, partner))
+    for dev in far:
         pl.semaphore_signal(ready_b, inc=1, device_id=dev, device_id_type=MESH)
 
     def take_pair(s):
@@ -337,71 +391,92 @@
     w_forward(4)
     queries(0, 0, theirs, 1)
     w_forward(5)
-    whole(crow.at[1], cs.at[0], cr.at[0]).wait_recv()
+    for i in range(2):
+        whole(crow.at[1 + i], cs.at[0], cr.at[i]).wait_recv()
     head_tables(1)
+    take_pair(1)
+    w_forward(6)
+    pass_recv(1, 1).wait_recv()
+    keys(1, 0, theirs, 1)
+    w_forward(7)
+    pl.semaphore_wait(ready_b, len(far))
     w_rest(0).wait_recv()
-    w_forward(6)
     keys(0, 1, 0, 2)
     state_out(0)
-    take_pair(1)
-    w_forward(7)
-    pass_recv(1, 1).wait_recv()
-    keys(1, 0, theirs, 1)
     keys(1, 1, 0, 2)
     state_out(1)
     keys(2, 1, mine, 1)
     keys(3, 1, mine, 1)
+    take_pair(2)
     queries(1, 0, theirs, 1)
-    take_pair(2)
     pass_recv(2, 1).wait_recv()
     keys(2, 0, theirs, 1)
     keys(2, 1, theirs, 1)
     state_out(2)
-    pl.semaphore_wait(ready_b, 2)
     state_row(0)
     state_row(1)
+    queries(2, 0, theirs, 1)
+    take_pair(3)
     w_rest(1).wait_recv()
     queries(0, 1, 0, 2)
-    take_pair(3)
-    queries(1, 1, 0, 2)
     pass_recv(3, 1).wait_recv()
     keys(3, 0, theirs, 1)
     keys(3, 1, theirs, 1)
     state_out(3)
-    queries(2, 0, theirs, 1)
+    queries(1, 1, 0, 2)
+    state_row(2)
+    state_back(0)
+    state_back(1)
     queries(2, 1, 0, 2)
-    state_row(2)
     queries(3, 0, theirs, 1)
+    state_row(3)
+    state_back(2)
+    state_back(3)
     queries(3, 1, 0, 2)
-    state_row(3)
-    for s in range(nseq):
-        state_back(s)
     for s in range(nseq):
         read_out(s)
     ow_load.wait()
-    whole(gat.at[:, :, 0:6 * HD], as_.at[0], ar.at[0]).wait_recv()
+    pg_load.wait()
+    whole(gat_early.at[:, 0:6 * HD], as_.at[0], ar.at[0]).wait_recv()
+    osc[...] = jnp.dot(gat_early[...], oww[...], preferred_element_type=F32)
+    scale_rows(osc, pg, mixed, 0, 2 * rows)
+    whole(gat_late.at[:, 0:6 * HD], as_.at[0], ar.at[1]).wait_recv()
 
     whole(raw, xs.at[0], xr.at[0]).wait_send()
     whole(tok.at[:, 0:2 * rows, :], ps.at[0], pr.at[0, 0]).wait_send()
     whole(w.at[1, :, 0:quarter, :], wxs.at[0], wxr.at[0]).wait_send()
     whole(w.at[1, :, 0:3 * quarter, :], wfs.at[0], wfr.at[0]).wait_send()
-    whole(crow.at[0], cs.at[0], cr.at[0]).wait_send()
-    whole(ybuf.at[:, pl.ds(0, 2 * ny - 1)], ys.at[0], yr.at[0]).wait_send()
-    whole(ybuf.at[:, pl.ds(0, 2 * ny - 1)], ms.at[0], mr.at[0]).wait_send()
-    whole(gat.at[:, :, 0:6 * HD], as_.at[0], ar.at[0]).wait_send()
-
-    @pl.loop(z + 1, nz)
-    def _(to):
-        whole(zsnd, zs.at[to], zr.at[0, to]).wait_send()
-
-
-def mix_kernel(gat, oww, pg, out_ref, osc):
+    whole(crow.at[0:2], cs.at[0], cr.at[0]).wait_send()
+    whole(gsend.at[:, pl.ds(0, 3 * rows), :], as_.at[0], ar.at[0]).wait_send()
+
+    @pl.when(core == 0)
+    def _():
+        whole(ybuf.at[:, pl.ds(0, 2 * ny)], ys.at[0], yr.at[0]).wait_send()
+
+    @pl.when(core == 1)
+    def _():
+        whole(ybuf.at[:, pl.ds(0, 2 * ny - 1)], ys.at[0], yr.at[0]).wait_send()
+        whole(ybuf.at[:, pl.ds(0, 4 * ny - 1)], ms.at[0], mr.at[0]).wait_send()
+
+        @pl.loop(z + 1, nz)
+        def _(to):
+            whole(zsnd, zs.at[to], zr.at[0, to]).wait_send()
+
+
+def mix_kernel(gat, oww, mixed, pg, out_ref, osc, late, sem):
+    done = mixed.shape[0]
+    first = pltpu.make_async_copy(mixed, out_ref.at[pl.ds(0, done), :], sem.at[0])
+    first.start()
     osc[...] = jnp.dot(gat[...], oww[...], preferred_element_type=F32)
-    width = osc.shape[1]
-    scale = row_scale(lambda c: osc[:, c * HD:(c + 1) * HD], width)
-    for c in range(width // HD):
-        cols = slice(c * HD, (c + 1) * HD)
-        out_ref[:, cols] = (osc[:, cols] * scale * pg[:, cols]).astype(BF16)
+    part = late.shape[0] // 2
+    copies = [first]
+    for i in range(2):
+        here = pl.ds(i * part, part)
+        scale_rows(osc, pg, late, i * part, part)
+        copies.append(pltpu.make_async_copy(late.at[here], out_ref.at[pl.ds(done + i * part, part), :], sem.at[1 + i]))
+        copies[-1].start()
+    for copy in copies:
+        copy.wait()
 
 
 def body(nz, ny, tokens, in_gain, wq, wk, wv, wg, log_decay, norm_gain, out_weight, post_gain):
@@ -419,8 +494,9 @@
         pltpu.VMEM((nseq, half, width), BF16),
         pltpu.VMEM((2, 2, width, 2 * HD), BF16),
         pltpu.VMEM((1, width), F32),
+        pltpu.VMEM((1, width), F32),
         pltpu.VMEM(tables.shape, F32),
-        pltpu.VMEM((2, 8, HD), F32),
+        pltpu.VMEM((3, 8, HD), F32),
         pltpu.VMEM((2, BLOCK, HD), F32),
         pltpu.VMEM((2, BLOCK, HD), F32),
         pltpu.VMEM((2, BLOCK, HD), F32),
@@ -433,46 +509,45 @@
         pltpu.VMEM((nseq, 2, half, HD), F32),
         pltpu.VMEM((nseq, 2, 2, HD, HD), F32),
         pltpu.VMEM((nseq, 2, HD, HD), BF16),
-        pltpu.VMEM((nseq, 2 * ny, qr, HD), BF16),
-        pltpu.VMEM((nseq, qr, HD), BF16),
-        pltpu.VMEM((nseq, nz, qr, HD), BF16),
-        pltpu.VMEM((nseq, 2 * ny, qr, HD), BF16),
+        pltpu.VMEM((nseq, 4 * ny, qr, HD), BF16),
+        pltpu.VMEM((nseq, 2, qr, HD), BF16),
+        pltpu.VMEM((nseq, nz, 2, qr, HD), BF16),
+        pltpu.VMEM((nseq, 4 * ny, qr, HD), BF16),
         pltpu.VMEM((nseq, 2, HD, HD), BF16),
         pltpu.VMEM((nseq, half, 2 * HD), BF16),
+        pltpu.VMEM((2 * rows, ntp * HD), BF16),
+        pltpu.VMEM((2 * rows, width), F32),
         dma((11,)),
         dma((1,)), dma((nseq,)), dma((1,)), dma((nseq, 2)), dma((1,)), dma((8,)), dma((1,)), dma((2,)),
-        dma((1,)), dma((1,)), dma((1,)), dma((nseq,)), dma((nz,)), dma((nseq, nz)), dma((1,)), dma((nseq,)),
-        dma((1,)), dma((1,)), signal, signal,
+        dma((1,)), dma((2,)), dma((1,)), dma((nseq,)), dma((nz,)), dma((nseq, nz)), dma((1,)), dma((nseq,)),
+        dma((1,)), dma((2,)), signal, signal,
     ]
-    gathered, weight = pl.pallas_call(
+    late = 2 * rows
+    gain = post_gain.reshape(1, -1)
+    gathered, weight, early = pl.pallas_call(
         functools.partial(kernel, nz, ny),
-        out_shape=[pltpu.VMEM((nseq, rows, ntp * HD), BF16), pltpu.VMEM(out_weight.shape, BF16)],
-        in_specs=[hbm] * 6 + [smem] + [hbm] * 3,
-        out_specs=[vmem, vmem],
+        out_shape=[
+            pltpu.VMEM((late, ntp * HD), BF16), pltpu.VMEM(out_weight.shape, BF16), pltpu.VMEM((late, width), BF16)
+        ],
+        in_specs=[hbm] * 6 + [smem] + [hbm] * 4,
+        out_specs=[vmem] * 3,
         scratch_shapes=scratch,
         name="retention",
         compiler_params=pltpu.CompilerParams(
-            collective_id=0, has_side_effects=True, vmem_limit_bytes=62_300_000
+            collective_id=0, has_side_effects=True, vmem_limit_bytes=VMEM_LIMIT
         ),
     )(
-        tokens, in_gain.reshape(1, -1), wq, wk, wv, wg, log_decay, norm_gain.reshape(1, -1), out_weight, tables,
+        tokens, in_gain.reshape(1, -1), wq, wk, wv, wg, log_decay, norm_gain.reshape(1, -1), out_weight, gain, tables,
     )
-    every = nseq * rows
-    step = every // 2
     mixed = pl.pallas_call(
         mix_kernel,
-        out_shape=jax.ShapeDtypeStruct((every, width), BF16),
-        grid=(every // step,),
-        in_specs=[
-            pl.BlockSpec((step, ntp * HD), lambda i: (i, 0)),
-            pl.BlockSpec(out_weight.shape, lambda i: (0, 0)),
-            pl.BlockSpec((1, width), lambda i: (0, 0)),
-        ],
-        out_specs=pl.BlockSpec((step, width), lambda i: (i, 0)),
-        scratch_shapes=[pltpu.VMEM((step, width), F32)],
+        out_shape=jax.ShapeDtypeStruct((nseq * rows, width), BF16),
+        in_specs=[vmem] * 4,
+        out_specs=hbm,
+        scratch_shapes=[pltpu.VMEM((late, width), F32), pltpu.VMEM((late, width), BF16), dma((3,))],
         name="mix",
         compiler_params=pltpu.CompilerParams(vmem_limit_bytes=16 * 1024 * 1024),
-    )(gathered.reshape(every, ntp * HD), weight, post_gain.reshape(1, -1))
+    )(gathered, weight, early, gain)
     return mixed.reshape(tokens.shape)
 
 

time: 55.4 us -> 52 us (0.939)
  Pallas kernels: 54.5 us -> 51.2 us
    pallas_call x1, Pallas kernels: 51.8 us -> 49.5 us  [body(): pl.pallas_call(functools.partial(kernel, nz, ny), out_shape=[pltpu.VMEM((...]
    pallas_call x1, Pallas kernels: 2.65 us -> 1.67 us  [body(): pl.pallas_call(mix_kernel, out_shape=jax.ShapeDtypeStruct((nseq * rows, w...]
where the time goes in v5:
time: 52 us; the launch traced here: 51.9 us
  Pallas kernels  51.2 us (98%)
  between operations  0.68 us (1%)
    pallas_call x1, Pallas kernels, body(): pl.pallas_call(functools.partial(kernel, nz, ny), out_shape=[pltpu.VMEM((...  49.5 us
    pallas_call x1, Pallas kernels, body(): pl.pallas_call(mix_kernel, out_shape=jax.ShapeDtypeStruct((nseq * rows, w...  1.67 us

profile of v5, /device:TPU:1, one launch (start us, length us, event | category | flops | bytes accessed | tf_op | source)
XLA Modules:
  0.0 51.9 jit_solution(10646885025933189648)
XLA Ops:
  0.0 0.0 copy-start
  0.7 49.5 %retention.1 = (bf16[128,1024]{1,0:T(8,128)(2,1)S(1)}, bf16[1024,2048]{1,0:T(8,128)(2,1)S(1)}, bf16[128,2048]{1,0:T(8,128)(2,1)S(1)}) custom-call(bf16[4,64,2048]{2,1,0:T(8,128)(2,1)} %tok_hbm.1, f32[1,2048]{1,0:T(1,128)} %bitcast.6, bf16[2048,128]{1,0:T(8,128)(2,1)} %wq.1, bf16[2048,128]{1,0:T(8,128)(2,1)} %wk.1, bf16[2048,128]{1,0:T(8,128)(2,1)} %wv.1, ...), custom_call_target="tpu_custom_call" | custom-call | tf_op jit(solution)/shard_map/retention/pallas_call | solution.py:527
  50.2 0.0 copy-done
  50.2 1.7 %mix.1 = bf16[256,2048]{1,0:T(8,128)(2,1)} custom-call(bf16[128,1024]{1,0:T(8,128)(2,1)S(1)} %get-tuple-element.8.gat, bf16[1024,2048]{1,0:T(8,128)(2,1)S(1)} %get-tuple-element.9.oww, bf16[128,2048]{1,0:T(8,128)(2,1)S(1)} %get-tuple-element.10.mixed, f32[1,2048]{1,0:T(1,128)S(1)} %bitcast.5), custom_call_target="tpu_custom_call" | custom-call | tf_op jit(solution)/shard_map/mix/pallas_call | solution.py:542
Async XLA Ops:
  0.0 50.2 %copy-start = (f32[2048]{0:T(1024)S(1)}, f32[2048]{0:T(1024)}, u32[]{:S(2)}) copy-start(f32[2048]{0:T(1024)} %param.20) | copy-start | bytes 24580

commit v6 on v5

--- a/solution.py
+++ b/solution.py
@@ -50,7 +50,7 @@
     nz, ny, tok_hbm, gain_hbm, wq, wk, wv, wg, ld_ref, ng_hbm, ow, pg_hbm, tab_hbm,
     gat_late, oww, mixed, raw, tok, w, gain, pg, tabs, crow, ctab, stab, dmat, qsc, ksc, kbuf, vbuf, qs, acc, gs, smat, esend, ybuf,
     zsnd, zbuf, msnd, mbuf, gsend, gat_early, osc, lsem, xs, xr, ps, pr, wxs, wxr, wfs, wfr, cs, cr, ys, yr, zs, zr, ms, mr, as_, ar,
-    ready_a, ready_b,
+    ready_a, ready_b, ready_c,
 ):
     nseq, rows, width = raw.shape
     ntp = 8
@@ -76,11 +76,21 @@
         return (zz + nz) % nz * ny + (yy + ny) % ny
 
     barrier = pltpu.get_barrier_semaphore()
-    near = [(at(z, y + k), me) for k in range(1, ny)] + [(at(z - 1, y), me), (at(z + 1, y), me), (sp, mate)]
-    near = near + [(sp, partner)]
-    peers = [(sp, pair_same), (sp, pair_other)] + near
-    for dev in peers:
-        pl.semaphore_signal(barrier, inc=1, device_id=dev, device_id_type=MESH)
+    plane = [(at(z, y + k), me) for k in range(1, ny)] + [(sp, mate), (sp, partner)]
+    beside = [(at(z - 1, y), me), (at(z + 1, y), me)]
+    beyond = [(at(z - 2, y), me), (at(z + 2, y), me)]
+    peers = [(sp, pair_same), (sp, pair_other)] + plane
+    even, odd = z % 2 == 0, z % 2 == 1
+
+    def tell(sem, devs):
+        for dev in devs:
+            pl.semaphore_signal(sem, inc=1, device_id=dev, device_id_type=MESH)
+
+    tell(barrier, peers)
+
+    @pl.when(even)
+    def _():
+        tell(barrier, beside)
 
     raw_loads = [pltpu.make_async_copy(tok_hbm.at[s], raw.at[s], lsem.at[s]) for s in range(nseq)]
     gain_load = pltpu.make_async_copy(gain_hbm, gain, lsem.at[4])
@@ -197,11 +207,22 @@
     ng_load.wait()
     crow[0, pl.ds(1, 7), :] = jnp.full((7, HD), ld_ref[0], F32)
 
-    pl.semaphore_wait(barrier, len(peers))
+    @pl.when(even)
+    def _():
+        pl.semaphore_wait(barrier, len(peers))
+
+    @pl.when(odd)
+    def _():
+        pl.semaphore_wait(barrier, len(peers) + 2)
+
     own_send(0).start()
     pass_send(0, 0).start()
-    for dev in near:
-        pl.semaphore_signal(ready_a, inc=1, device_id=dev, device_id_type=MESH)
+    tell(ready_a, plane)
+
+    @pl.when(odd)
+    def _():
+        tell(ready_a, beside)
+
     c_send(0).start()
     c_send(1).start()
     for c in range(2):
@@ -370,10 +391,16 @@
         keys(s, 0, mine, 1)
         queries(s, 0, mine, 1)
 
-    pl.semaphore_wait(ready_a, len(near))
-    far = ((at(z - 2, y), me), (at(z + 2, y), me), (sp, partner))
-    for dev in far:
-        pl.semaphore_signal(ready_b, inc=1, device_id=dev, device_id_type=MESH)
+    @pl.when(even)
+    def _():
+        pl.semaphore_wait(ready_a, len(plane) + 2)
+        tell(ready_b, beyond)
+
+    @pl.when(odd)
+    def _():
+        pl.semaphore_wait(ready_a, len(plane))
+
+    tell(ready_b, [(sp, partner)])
 
     def take_pair(s):
         own_recv(s).wait_recv()
@@ -399,7 +426,15 @@
     pass_recv(1, 1).wait_recv()
     keys(1, 0, theirs, 1)
     w_forward(7)
-    pl.semaphore_wait(ready_b, len(far))
+    @pl.when(even)
+    def _():
+        pl.semaphore_wait(ready_b, 3)
+        tell(ready_c, beside)
+
+    @pl.when(odd)
+    def _():
+        pl.semaphore_wait(ready_b, 1)
+
     w_rest(0).wait_recv()
     keys(0, 1, 0, 2)
     state_out(0)
@@ -413,6 +448,10 @@
     keys(2, 0, theirs, 1)
     keys(2, 1, theirs, 1)
     state_out(2)
+    @pl.when(odd)
+    def _():
+        pl.semaphore_wait(ready_c, 2)
+
     state_row(0)
     state_row(1)
     queries(2, 0, theirs, 1)
@@ -520,7 +559,7 @@
         dma((11,)),
         dma((1,)), dma((nseq,)), dma((1,)), dma((nseq, 2)), dma((1,)), dma((8,)), dma((1,)), dma((2,)),
         dma((1,)), dma((2,)), dma((1,)), dma((nseq,)), dma((nz,)), dma((nseq, nz)), dma((1,)), dma((nseq,)),
-        dma((1,)), dma((2,)), signal, signal,
+        dma((1,)), dma((2,)), signal, signal, signal,
     ]
     late = 2 * rows
     gain = post_gain.reshape(1, -1)

time: 52 us -> 49.2 us (0.946)
  Pallas kernels: 51.2 us -> 48.4 us
    pallas_call x1, Pallas kernels: 49.5 us -> 46.7 us  [body(): pl.pallas_call(functools.partial(kernel, nz, ny), out_shape=[pltpu.VMEM((...]
where the time goes in v6:
time: 49.2 us; the launch traced here: 49.1 us
  Pallas kernels  48.4 us (98%)
  between operations  0.68 us (1%)
    pallas_call x1, Pallas kernels, body(): pl.pallas_call(functools.partial(kernel, nz, ny), out_shape=[pltpu.VMEM((...  46.7 us
    pallas_call x1, Pallas kernels, body(): pl.pallas_call(mix_kernel, out_shape=jax.ShapeDtypeStruct((nseq * rows, w...  1.67 us

profile of v6, /device:TPU:1, one launch (start us, length us, event | category | flops | bytes accessed | tf_op | source)
XLA Modules:
  0.0 49.1 jit_solution(500727701874499432)
XLA Ops:
  0.0 0.0 copy-start
  0.7 46.7 %retention.1 = (bf16[128,1024]{1,0:T(8,128)(2,1)S(1)}, bf16[1024,2048]{1,0:T(8,128)(2,1)S(1)}, bf16[128,2048]{1,0:T(8,128)(2,1)S(1)}) custom-call(bf16[4,64,2048]{2,1,0:T(8,128)(2,1)} %tok_hbm.1, f32[1,2048]{1,0:T(1,128)} %bitcast.6, bf16[2048,128]{1,0:T(8,128)(2,1)} %wq.1, bf16[2048,128]{1,0:T(8,128)(2,1)} %wk.1, bf16[2048,128]{1,0:T(8,128)(2,1)} %wv.1, ...), custom_call_target="tpu_custom_call" | custom-call | tf_op jit(solution)/shard_map/retention/pallas_call | solution.py:566
  47.4 0.0 copy-done
  47.4 1.7 %mix.1 = bf16[256,2048]{1,0:T(8,128)(2,1)} custom-call(bf16[128,1024]{1,0:T(8,128)(2,1)S(1)} %get-tuple-element.8.gat, bf16[1024,2048]{1,0:T(8,128)(2,1)S(1)} %get-tuple-element.9.oww, bf16[128,2048]{1,0:T(8,128)(2,1)S(1)} %get-tuple-element.10.mixed, f32[1,2048]{1,0:T(1,128)S(1)} %bitcast.5), custom_call_target="tpu_custom_call" | custom-call | tf_op jit(solution)/shard_map/mix/pallas_call | solution.py:581
Async XLA Ops:
  0.0 47.4 %copy-start = (f32[2048]{0:T(1024)S(1)}, f32[2048]{0:T(1024)}, u32[]{:S(2)}) copy-start(f32[2048]{0:T(1024)} %param.20) | copy-start | bytes 24580

commit v7 on v6

--- a/solution.py
+++ b/solution.py
@@ -171,11 +171,7 @@
         return remote(src, dst, ys.at[0], yr.at[s], (at(z, to), owners[k]))
 
     def zcopy(s, to):
-        return remote(zsnd.at[s], zbuf.at[s, z], zs.at[to], zr.at[s, z], (to * ny + y, me))
-
-    def zrecv(s, frm):
-        ref = zbuf.at[s, frm]
-        return remote(ref, ref, zs.at[frm], zr.at[s, frm], (frm * ny + y, me))
+        return remote(zsnd.at[s], zbuf.at[s, z], zs.at[0], zr.at[s], (to * ny + y, me))
 
     def mcopy(s, i, k, to):
         src = msnd.at[s, i * 2 * ny + to * 2 + (half, 1 - half)[k]]
@@ -342,8 +338,12 @@
             steps = [owned_decay(i, float(span)) for i in range(2)]
             row_steps = [owned_decay(i, float(span * 2 * ny)) for i in range(2)]
 
+            for count in range(1, nz):
+                @pl.when(z == count)
+                def _():
+                    whole(zbuf.at[s, pl.ds(0, count)], zs.at[0], zr.at[s]).wait_recv()
+
             def add(frm, totals):
-                zrecv(s, frm).wait_recv()
                 return tuple(totals[i] * row_steps[i] + zbuf[s, frm, i].astype(F32) for i in range(2))
 
             zero = jnp.zeros((qr, HD), F32)
@@ -380,8 +380,8 @@
                 spread = jnp.mean(kept * kept, axis=-1, keepdims=True)
                 kept = kept * lax.rsqrt(spread + GROUP_EPS) * gs[s, k, here, :]
                 gsend[s, here, k * HD:(k + 1) * HD] = kept.astype(BF16)
-        for k in range(1, 4):
-            acopy(s, (dl + k) % 4).start()
+        for to in (theirs * 2 + core, theirs * 2 + 1 - core, mine * 2 + 1 - core):
+            acopy(s, to).start()
         own = gsend[s, pl.ds(pl.multiple_of(dl * rows, rows), rows), :]
         gat_of(s)[:, pl.ds(pl.multiple_of(dl * 2 * HD, 2 * HD), 2 * HD)] = own
 
@@ -470,12 +470,14 @@
     queries(3, 0, theirs, 1)
     state_row(3)
     state_back(2)
+    queries(3, 1, 0, 2)
     state_back(3)
-    queries(3, 1, 0, 2)
-    for s in range(nseq):
-        read_out(s)
+    read_out(0)
+    read_out(1)
+    read_out(2)
     ow_load.wait()
     pg_load.wait()
+    read_out(3)
     whole(gat_early.at[:, 0:6 * HD], as_.at[0], ar.at[0]).wait_recv()
     osc[...] = jnp.dot(gat_early[...], oww[...], preferred_element_type=F32)
     scale_rows(osc, pg, mixed, 0, 2 * rows)
@@ -497,9 +499,10 @@
         whole(ybuf.at[:, pl.ds(0, 2 * ny - 1)], ys.at[0], yr.at[0]).wait_send()
         whole(ybuf.at[:, pl.ds(0, 4 * ny - 1)], ms.at[0], mr.at[0]).wait_send()
 
-        @pl.loop(z + 1, nz)
-        def _(to):
-            whole(zsnd, zs.at[to], zr.at[0, to]).wait_send()
+        for count in range(1, nz):
+            @pl.when(z == nz - 1 - count)
+            def _():
+                whole(zbuf.at[:, pl.ds(0, count)], zs.at[0], zr.at[0]).wait_send()
 
 
 def mix_kernel(gat, oww, mixed, pg, out_ref, osc, late, sem):
@@ -558,7 +561,7 @@
         pltpu.VMEM((2 * rows, width), F32),
         dma((11,)),
         dma((1,)), dma((nseq,)), dma((1,)), dma((nseq, 2)), dma((1,)), dma((8,)), dma((1,)), dma((2,)),
-        dma((1,)), dma((2,)), dma((1,)), dma((nseq,)), dma((nz,)), dma((nseq, nz)), dma((1,)), dma((nseq,)),
+        dma((1,)), dma((2,)), dma((1,)), dma((nseq,)), dma((1,)), dma((nseq,)), dma((1,)), dma((nseq,)),
         dma((1,)), dma((2,)), signal, signal, signal,
     ]
     late = 2 * rows

time: 49.2 us -> 48.8 us (level)
  no operation moved by 1% of the time
where the time goes in v7:
time: 48.8 us; the launch traced here: 48.7 us
  Pallas kernels  48 us (98%)
  between operations  0.68 us (1%)
    pallas_call x1, Pallas kernels, body(): pl.pallas_call(functools.partial(kernel, nz, ny), out_shape=[pltpu.VMEM((...  46.4 us
    pallas_call x1, Pallas kernels, body(): pl.pallas_call(mix_kernel, out_shape=jax.ShapeDtypeStruct((nseq * rows, w...  1.67 us

profile of v7, /device:TPU:1, one launch (start us, length us, event | category | flops | bytes accessed | tf_op | source)
XLA Modules:
  0.0 48.7 jit_solution(1601097754808156390)
XLA Ops:
  0.0 0.0 copy-start
  0.7 46.4 %retention.1 = (bf16[128,1024]{1,0:T(8,128)(2,1)S(1)}, bf16[1024,2048]{1,0:T(8,128)(2,1)S(1)}, bf16[128,2048]{1,0:T(8,128)(2,1)S(1)}) custom-call(bf16[4,64,2048]{2,1,0:T(8,128)(2,1)} %tok_hbm.1, f32[1,2048]{1,0:T(1,128)} %bitcast.6, bf16[2048,128]{1,0:T(8,128)(2,1)} %wq.1, bf16[2048,128]{1,0:T(8,128)(2,1)} %wk.1, bf16[2048,128]{1,0:T(8,128)(2,1)} %wv.1, ...), custom_call_target="tpu_custom_call" | custom-call | tf_op jit(solution)/shard_map/retention/pallas_call | solution.py:569
  47.1 0.0 copy-done
  47.1 1.7 %mix.1 = bf16[256,2048]{1,0:T(8,128)(2,1)} custom-call(bf16[128,1024]{1,0:T(8,128)(2,1)S(1)} %get-tuple-element.8.gat, bf16[1024,2048]{1,0:T(8,128)(2,1)S(1)} %get-tuple-element.9.oww, bf16[128,2048]{1,0:T(8,128)(2,1)S(1)} %get-tuple-element.10.mixed, f32[1,2048]{1,0:T(1,128)S(1)} %bitcast.5), custom_call_target="tpu_custom_call" | custom-call | tf_op jit(solution)/shard_map/mix/pallas_call | solution.py:584
Async XLA Ops:
  0.0 47.1 %copy-start = (f32[2048]{0:T(1024)S(1)}, f32[2048]{0:T(1024)}, u32[]{:S(2)}) copy-start(f32[2048]{0:T(1024)} %param.20) | copy-start | bytes 24580

commit v8 on v7

--- a/solution.py
+++ b/solution.py
@@ -411,7 +411,10 @@
     w_forward(1)
     w_forward(2)
     take_pair(0)
-    own_send(3).start()
+    @pl.when(core == 0)
+    def _():
+        own_send(3).start()
+
     w_forward(3)
     pass_recv(0, 1).wait_recv()
     keys(0, 0, theirs, 1)
@@ -438,6 +441,11 @@
     w_rest(0).wait_recv()
     keys(0, 1, 0, 2)
     state_out(0)
+
+    @pl.when(core == 1)
+    def _():
+        own_send(3).start()
+
     keys(1, 1, 0, 2)
     state_out(1)
     keys(2, 1, mine, 1)

time: 48.8 us -> 48.8 us (level)
  no operation moved by 1% of the time
where the time goes in v8:
time: 48.8 us; the launch traced here: 48.7 us
  Pallas kernels  48 us (98%)
  between operations  0.68 us (1%)
    pallas_call x1, Pallas kernels, body(): pl.pallas_call(functools.partial(kernel, nz, ny), out_shape=[pltpu.VMEM((...  46.4 us
    pallas_call x1, Pallas kernels, body(): pl.pallas_call(mix_kernel, out_shape=jax.ShapeDtypeStruct((nseq * rows, w...  1.67 us

profile of v8, /device:TPU:1, one launch (start us, length us, event | category | flops | bytes accessed | tf_op | source)
XLA Modules:
  0.0 48.7 jit_solution(17396220398125692816)
XLA Ops:
  0.0 0.0 copy-start
  0.7 46.4 %retention.1 = (bf16[128,1024]{1,0:T(8,128)(2,1)S(1)}, bf16[1024,2048]{1,0:T(8,128)(2,1)S(1)}, bf16[128,2048]{1,0:T(8,128)(2,1)S(1)}) custom-call(bf16[4,64,2048]{2,1,0:T(8,128)(2,1)} %tok_hbm.1, f32[1,2048]{1,0:T(1,128)} %bitcast.6, bf16[2048,128]{1,0:T(8,128)(2,1)} %wq.1, bf16[2048,128]{1,0:T(8,128)(2,1)} %wk.1, bf16[2048,128]{1,0:T(8,128)(2,1)} %wv.1, ...), custom_call_target="tpu_custom_call" | custom-call | tf_op jit(solution)/shard_map/retention/pallas_call | solution.py:577
  47.0 0.0 copy-done
  47.1 1.7 %mix.1 = bf16[256,2048]{1,0:T(8,128)(2,1)} custom-call(bf16[128,1024]{1,0:T(8,128)(2,1)S(1)} %get-tuple-element.8.gat, bf16[1024,2048]{1,0:T(8,128)(2,1)S(1)} %get-tuple-element.9.oww, bf16[128,2048]{1,0:T(8,128)(2,1)S(1)} %get-tuple-element.10.mixed, f32[1,2048]{1,0:T(1,128)S(1)} %bitcast.5), custom_call_target="tpu_custom_call" | custom-call | tf_op jit(solution)/shard_map/mix/pallas_call | solution.py:592
Async XLA Ops:
  0.0 47.0 %copy-start = (f32[2048]{0:T(1024)S(1)}, f32[2048]{0:T(1024)}, u32[]{:S(2)}) copy-start(f32[2048]{0:T(1024)} %param.20) | copy-start | bytes 24580

commit v9 on v7

--- a/solution.py
+++ b/solution.py
@@ -299,11 +299,16 @@
         if to != ny // 2:
             far_first.append((0, to))
 
-    def state_out(s):
-        for k in range(2):
-            esend[s, k] = (smat[s, k, 0] * decay(k, float(BLOCK)) + smat[s, k, 1]).astype(BF16)
-        for k, to in far_first:
-            ycopy(s, k, (y + to) % ny).start()
+    def state_head(s, k):
+        esend[s, k] = (smat[s, k, 0] * decay(k, float(BLOCK)) + smat[s, k, 1]).astype(BF16)
+        for head, to in far_first:
+            if head == k:
+                ycopy(s, k, (y + to) % ny).start()
+
+    def state_out(s, last=False):
+        if not last:
+            state_head(s, 1)
+        state_head(s, 0)
 
         @pl.when(core == 0)
         def _():
@@ -459,9 +464,10 @@
     w_rest(1).wait_recv()
     queries(0, 1, 0, 2)
     pass_recv(3, 1).wait_recv()
+    keys(3, 1, theirs, 1)
+    state_head(3, 1)
     keys(3, 0, theirs, 1)
-    keys(3, 1, theirs, 1)
-    state_out(3)
+    state_out(3, True)
     queries(1, 1, 0, 2)
     state_row(2)
     state_back(0)

time: 48.8 us -> 48.8 us (level)
  no operation moved by 1% of the time
where the time goes in v9:
time: 48.8 us; the launch traced here: 48.7 us
  Pallas kernels  48 us (98%)
  between operations  0.68 us (1%)
    pallas_call x1, Pallas kernels, body(): pl.pallas_call(functools.partial(kernel, nz, ny), out_shape=[pltpu.VMEM((...  46.3 us
    pallas_call x1, Pallas kernels, body(): pl.pallas_call(mix_kernel, out_shape=jax.ShapeDtypeStruct((nseq * rows, w...  1.67 us

profile of v9, /device:TPU:1, one launch (start us, length us, event | category | flops | bytes accessed | tf_op | source)
XLA Modules:
  0.0 48.7 jit_solution(2011569323886673414)
XLA Ops:
  0.0 0.0 copy-start
  0.7 46.3 %retention.1 = (bf16[128,1024]{1,0:T(8,128)(2,1)S(1)}, bf16[1024,2048]{1,0:T(8,128)(2,1)S(1)}, bf16[128,2048]{1,0:T(8,128)(2,1)S(1)}) custom-call(bf16[4,64,2048]{2,1,0:T(8,128)(2,1)} %tok_hbm.1, f32[1,2048]{1,0:T(1,128)} %bitcast.6, bf16[2048,128]{1,0:T(8,128)(2,1)} %wq.1, bf16[2048,128]{1,0:T(8,128)(2,1)} %wk.1, bf16[2048,128]{1,0:T(8,128)(2,1)} %wv.1, ...), custom_call_target="tpu_custom_call" | custom-call | tf_op jit(solution)/shard_map/retention/pallas_call | solution.py:575
  47.0 0.0 copy-done
  47.0 1.7 %mix.1 = bf16[256,2048]{1,0:T(8,128)(2,1)} custom-call(bf16[128,1024]{1,0:T(8,128)(2,1)S(1)} %get-tuple-element.8.gat, bf16[1024,2048]{1,0:T(8,128)(2,1)S(1)} %get-tuple-element.9.oww, bf16[128,2048]{1,0:T(8,128)(2,1)S(1)} %get-tuple-element.10.mixed, f32[1,2048]{1,0:T(1,128)S(1)} %bitcast.5), custom_call_target="tpu_custom_call" | custom-call | tf_op jit(solution)/shard_map/mix/pallas_call | solution.py:590
Async XLA Ops:
  0.0 47.0 %copy-start = (f32[2048]{0:T(1024)S(1)}, f32[2048]{0:T(1024)}, u32[]{:S(2)}) copy-start(f32[2048]{0:T(1024)} %param.20) | copy-start | bytes 24580
